TPU v7x, 32 devices: a whole 2x2x4 slice. The times are simulated.
32 devices in a mesh: sp: 8 (over z, y), tp: 4 (over x, core).
Axes of the slice: x: 2, y: 2, z: 4, core: 2. Of those that a mesh axis runs over, the one named last changes fastest.
Arguments:
- queries: bfloat16 [8192, 1024], P('sp', 'tp'), may hold values from -6 to 6
- cell_key_rows: bfloat16 [8192, 1024], P('sp', 'tp'), may hold values from -6 to 6
- cell_value_rows: bfloat16 [8192, 2048], P('sp', 'tp'), may hold values from -6 to 6
- output_gate_logits: bfloat16 [8192, 2048], P('sp', 'tp'), may hold values from -6 to 6
- input_gate_logits: bfloat16 [8, 8192], P('tp', 'sp'), may hold values from -4 to 216
- forget_gate_logits: bfloat16 [8, 8192], P('tp', 'sp'), may hold values from 0.5 to 14
- forget_extra_term: float32 [8, 8192], P('tp', 'sp'), may hold values from -1.4 to 0
- residual: bfloat16 [8192, 2048], P('sp', 'tp'), may hold values from -13 to 13
- head_norm_gain: bfloat16 [2048], P('tp'), may hold values from 0.099609375 to 1.8984375
- cell_output_weight: bfloat16 [2048, 2048], P('tp'), may hold values from -0.25 to 0.25
- feedforward_norm_gain: bfloat16 [2048], replicated, may hold values from 0.099609375 to 1.8984375
- gate_projection_weight: bfloat16 [2048, 5632], P('sp', 'tp'), may hold values from -0.125 to 0.125
- up_projection_weight: bfloat16 [2048, 5632], P('sp', 'tp'), may hold values from -0.125 to 0.125
- down_projection_weight: bfloat16 [5632, 2048], P('tp', 'sp'), may hold values from -0.15625 to 0.15625
Outputs:
- mixed: bfloat16 [8192, 2048], P('sp', 'tp')
All inputs are finite; a program needn't handle non-finite values.
Results may differ from a plain program's by a relative error of at most 0.017.
Values may be sent and summed in bfloat16 or wider, within the bound.
A program may use at most 128 MiB of HBM per device.

v0:
```python
import jax
import jax.numpy as jnp
from jax import lax
from jax.experimental import pallas as pl
from jax.experimental.pallas import tpu as pltpu
from jax.sharding import PartitionSpec as P

LOWEST_LOG = -1e30
EPSILON = 1e-06


def shift_pairs(length, step):
    return [(source, source + step) for source in range(length - step)]


def entering_state(state, top, total):
    length, index = lax.axis_size("sp"), lax.axis_index("sp")
    heads, key_width, value_width = state.shape

    def pack(s, t, f):
        tail = jnp.zeros((heads, 8, value_width), jnp.float32)
        tail = tail.at[:, 0, :].set(t[:, None]).at[:, 1, :].set(f[:, None])
        return jnp.concatenate([s, tail], axis=1)

    def unpack(p, valid):
        s = p[:, :key_width, :]
        t = jnp.where(valid, p[:, key_width, 0], LOWEST_LOG)
        f = jnp.where(valid, p[:, key_width + 1, 0], 0.0)
        return jnp.where(valid, s, 0.0), t, f

    moved = lax.ppermute(pack(state, top, total), "sp", shift_pairs(length, 1))
    s, t, f = unpack(moved, index >= 1)
    step = 1
    while step < length - 1:
        moved = lax.ppermute(pack(s, t, f), "sp", shift_pairs(length, step))
        s0, t0, f0 = unpack(moved, index >= step)
        from_top = t0 + f
        new_top = jnp.maximum(from_top, t)
        s = (
            jnp.exp(from_top - new_top)[:, None, None] * s0
            + jnp.exp(t - new_top)[:, None, None] * s
        )
        t, f = new_top, f0 + f
        step *= 2
    return s, t


def cell_kernel(q_ref, k_ref, v_ref, a_ref, m_ref, c_ref, state_ref, open_ref, gain_ref, o_ref, *, scale):
    block = q_ref.shape[0]
    length = k_ref.shape[0]
    q = q_ref[...]
    first = pl.program_id(1) * block
    scores = lax.dot_general(
        q, k_ref[...], (((1,), (1,)), ((), ())), preferred_element_type=jnp.float32
    )
    rows = first + lax.broadcasted_iota(jnp.int32, (block, length), 0)
    cols = lax.broadcasted_iota(jnp.int32, (block, length), 1)
    weight = jnp.where(cols <= rows, jnp.exp(jnp.minimum(a_ref[0] - m_ref[0], 0.0)), 0.0)
    numer = jnp.dot(
        (scores * weight).astype(jnp.bfloat16), v_ref[...], preferred_element_type=jnp.float32
    )
    before = jnp.dot(q, state_ref[0].astype(jnp.bfloat16), preferred_element_type=jnp.float32)
    memory = (numer + c_ref[0] * before) * scale
    normal = memory * lax.rsqrt(jnp.mean(memory * memory, axis=-1, keepdims=True) + EPSILON)
    gate_open = jax.nn.sigmoid(open_ref[...].astype(jnp.float32))
    o_ref[...] = (normal * gain_ref[...].astype(jnp.float32) * gate_open).astype(o_ref.dtype)


def cell(queries, keys, values, a_log, m_col, c_col, state, open_logits, gain):
    heads, length = a_log.shape
    dk, dv = queries.shape[1] // heads, values.shape[1] // heads
    block = min(length, 256)
    return pl.pallas_call(
        lambda *refs: cell_kernel(*refs, scale=dk ** (-0.5)),
        grid=(heads, length // block),
        in_specs=[
            pl.BlockSpec((block, dk), lambda h, i: (i, h)),
            pl.BlockSpec((length, dk), lambda h, i: (0, h)),
            pl.BlockSpec((length, dv), lambda h, i: (0, h)),
            pl.BlockSpec((1, 1, length), lambda h, i: (h, 0, 0)),
            pl.BlockSpec((1, block, 1), lambda h, i: (h, i, 0)),
            pl.BlockSpec((1, block, 1), lambda h, i: (h, i, 0)),
            pl.BlockSpec((1, dk, dv), lambda h, i: (h, 0, 0)),
            pl.BlockSpec((block, dv), lambda h, i: (i, h)),
            pl.BlockSpec((1, dv), lambda h, i: (0, h)),
        ],
        out_specs=pl.BlockSpec((block, dv), lambda h, i: (i, h)),
        out_shape=jax.ShapeDtypeStruct((length, heads * dv), jnp.bfloat16),
        cost_estimate=pl.CostEstimate(
            flops=8 * heads * length * length * dv, bytes_accessed=6 * length * heads * dv, transcendentals=0
        ),
        name="cell",
    )(queries, keys, values, a_log[:, None, :], m_col[:, :, None], c_col[:, :, None], state, open_logits, gain)


def partner_pairs(count):
    return [(i, i ^ 1) for i in range(count)]


def ring_pairs(count, step):
    return [(i, (i + 2 * step) % count) for i in range(count)]


def product_scattered(rows, weight):
    count, index = lax.axis_size("tp"), lax.axis_index("tp")
    chips, core, chip = count // 2, index % 2, index // 2
    width = weight.shape[1] // count

    def product(block):
        columns = lax.dynamic_slice_in_dim(weight, block * width, width, 1)
        return jnp.dot(rows, columns, preferred_element_type=jnp.float32)

    def chip_sum(to):
        given = product(2 * to + 1 - core).astype(jnp.bfloat16)
        got = lax.ppermute(given, "tp", partner_pairs(count))
        return product(2 * to + core) + got.astype(jnp.float32)

    moved = []
    for step in range(1, chips):
        sent = chip_sum((chip + step) % chips).astype(jnp.bfloat16)
        moved.append(lax.ppermute(sent, "tp", ring_pairs(count, step)))
    total = chip_sum(chip)
    for part in moved:
        total = total + part.astype(jnp.float32)
    return total


def columns_gathered(block):
    count, index = lax.axis_size("tp"), lax.axis_index("tp")
    chips, core, chip = count // 2, index % 2, index // 2
    width = block.shape[1]
    whole = jnp.zeros((block.shape[0], count * width), block.dtype)
    held = [(chip, block)]
    for step in range(1, chips):
        moved = lax.ppermute(block, "tp", ring_pairs(count, step))
        held.append(((chip - step) % chips, moved))
    for place, piece in held:
        other = lax.ppermute(piece, "tp", partner_pairs(count))
        whole = lax.dynamic_update_slice(whole, piece, (0, (2 * place + core) * width))
        whole = lax.dynamic_update_slice(whole, other, (0, (2 * place + 1 - core) * width))
    return whole


def local(
    queries,
    cell_key_rows,
    cell_value_rows,
    output_gate_logits,
    input_gate_logits,
    forget_gate_logits,
    forget_extra_term,
    residual,
    head_norm_gain,
    cell_output_weight,
    feedforward_norm_gain,
    gate_projection_weight,
    up_projection_weight,
    down_projection_weight,
):
    whole_gate = lax.all_gather(gate_projection_weight, "sp", axis=0, tiled=True)
    whole_up = lax.all_gather(up_projection_weight, "sp", axis=0, tiled=True)
    length = queries.shape[0]
    heads = input_gate_logits.shape[0]
    dk, dv = queries.shape[1] // heads, cell_value_rows.shape[1] // heads
    log_forget = jax.nn.log_sigmoid(forget_gate_logits.astype(jnp.float32)) + forget_extra_term
    running = jnp.cumsum(log_forget, axis=-1)
    a_log = input_gate_logits.astype(jnp.float32) - running
    m_log = lax.cummax(a_log, axis=1)
    a_top, total = m_log[:, -1], running[:, -1]
    decay = jnp.exp(a_log - a_top[:, None])
    weighed = (
        cell_key_rows.reshape(length, heads, dk).astype(jnp.float32) * decay.T[:, :, None]
    ).astype(jnp.bfloat16)
    state = jnp.stack(
        [
            lax.dot_general(
                weighed[:, h],
                cell_value_rows[:, h * dv : (h + 1) * dv],
                (((0,), (0,)), ((), ())),
                preferred_element_type=jnp.float32,
            )
            for h in range(heads)
        ]
    )
    carried, carried_top = entering_state(state, a_top + total, total)
    m_all = jnp.maximum(m_log, carried_top[:, None])
    coefficient = jnp.exp(carried_top[:, None] - m_all)
    gated = cell(
        queries,
        cell_key_rows,
        cell_value_rows,
        a_log,
        m_all,
        coefficient,
        carried,
        output_gate_logits,
        head_norm_gain[None, :],
    )
    summed = product_scattered(gated, cell_output_weight)
    stream = (residual.astype(jnp.float32) + summed).astype(jnp.bfloat16)
    down_late, stream = lax.optimization_barrier((down_projection_weight, stream))
    whole_down = lax.all_gather(down_late, "sp", axis=1, tiled=True)
    wide = columns_gathered(stream).astype(jnp.float32)
    scale = lax.rsqrt(jnp.mean(wide * wide, axis=-1, keepdims=True) + EPSILON)
    normed = (wide * scale * feedforward_norm_gain.astype(jnp.float32)[None, :]).astype(jnp.bfloat16)
    gate_value = jnp.dot(normed, whole_gate, preferred_element_type=jnp.float32)
    lifted = jnp.dot(normed, whole_up, preferred_element_type=jnp.float32)
    hidden = (jax.nn.silu(gate_value) * lifted).astype(jnp.bfloat16)
    channel_total = product_scattered(hidden, whole_down)
    return (stream.astype(jnp.float32) + 0.5 * channel_total).astype(jnp.bfloat16)


def solution(mesh):
    placed = (
        P("sp", "tp"),
        P("sp", "tp"),
        P("sp", "tp"),
        P("sp", "tp"),
        P("tp", "sp"),
        P("tp", "sp"),
        P("tp", "sp"),
        P("sp", "tp"),
        P("tp"),
        P("tp", None),
        P(),
        P("sp", "tp"),
        P("sp", "tp"),
        P("tp", "sp"),
    )
    return jax.shard_map(
        local, mesh=mesh, in_specs=placed, out_specs=P("sp", "tp"), check_vma=False
    )
```

profile of v0, /device:TPU:24, one launch (start us, length us, event | category | flops | bytes accessed | tf_op | source)
XLA Modules:
  0.0 353.5 jit_solution(13519535385364474644)
XLA Ops:
  6.5 0.7 all-gather.4.cloned.1.call-update
  7.3 0.7 all-gather.6.cloned.1.call-update
  8.1 0.7 fusion.33
  8.8 0.6 reduce-window.14
  9.8 0.7 convert_subtract_fusion
  11.8 1.3 copy.21
  13.4 1.3 convolution_bitcast_fusion
  14.7 1.3 convolution_bitcast_fusion.1
  16.0 3.4 collective-permute-start
  19.4 20.8 %collective-permute-done = f32[2,136,256]{2,1,0:T(8,128)S(1)} collective-permute-done((f32[2,136,256]{2,1,0:T(8,128)S(1)}, f32[2,136,256]{2,1,0:T(8,128)S(1)}, u32[]{:S(2)}, u32[]{:S(2)}) %collective-permute-start) | collective-permute-done | bytes 278560 | tf_op jit(solution)/shard_map/ppermute | solution.py:31
  40.6 1.9 collective-permute-start.1
  42.5 13.8 %collective-permute-done.1 = f32[2,136,256]{2,1,0:T(8,128)S(1)} collective-permute-done((f32[2,136,256]{2,1,0:T(8,128)S(1)}, f32[2,136,256]{2,1,0:T(8,128)S(1)}, u32[]{:S(2)}, u32[]{:S(2)}) %collective-permute-start.1) | collective-permute-done | bytes 278560 | tf_op jit(solution)/shard_map/ppermute | solution.py:35
  56.8 1.3 collective-permute-start.2
  58.1 19.5 %collective-permute-done.2 = f32[2,136,256]{2,1,0:T(8,128)} collective-permute-done((f32[2,136,256]{2,1,0:T(8,128)S(1)}, f32[2,136,256]{2,1,0:T(8,128)}, u32[]{:S(2)}, u32[]{:S(2)}) %collective-permute-start.2) | collective-permute-done | bytes 278560 | tf_op jit(solution)/shard_map/ppermute | solution.py:35
  77.6 0.9 fusion.48
  78.8 1.1 fusion.28
  79.8 0.7 pad_maximum_fusion.3
  80.5 1.5 collective-permute-start.3
  82.0 0.6 broadcast_in_dim.25.refs_3_
  82.7 0.9 reduce_window_max.31
  84.2 29.3 %collective-permute-done.3 = f32[2,136,256]{2,1,0:T(8,128)} collective-permute-done((f32[2,136,256]{2,1,0:T(8,128)}, f32[2,136,256]{2,1,0:T(8,128)}, u32[]{:S(2)}, u32[]{:S(2)}) %collective-permute-start.3) | collective-permute-done | bytes 278560 | tf_op jit(solution)/shard_map/ppermute | solution.py:35
  113.5 0.8 add_add_fusion
  114.4 1.8 fusion.26.refs_6_
  116.2 1.5 subtract_exponential_fusion
  117.7 9.1 %cell.1 = bf16[1024,512]{1,0:T(8,128)(2,1)} custom-call(bf16[1024,256]{1,0:T(8,128)(2,1)} %refs_0_.1, bf16[1024,256]{1,0:T(8,128)(2,1)} %refs_1_.1, bf16[1024,512]{1,0:T(8,128)(2,1)} %refs_2_.1, f32[2,1,1024]{2,1,0:T(1,128)} %broadcast_in_dim.25.refs_3_, f32[2,1024,1]{2,1,0:T(8,128)} %get-tuple-element.123.refs_4_, ...), custom_call_target="tpu_custom_call" | custom-call | flops 4294967296 | bytes 3145728 | tf_op jit(solution)/shard_map/cell/pallas_call | solution.py:73
  126.8 3.0 convolution_convert_fusion.2
  129.8 3.0 convolution_convert_fusion.3
  133.3 2.9 add_convert_fusion.3
  136.3 3.2 collective-permute-start.6
  139.4 0.7 fusion.21
  140.2 22.9 %collective-permute-done.6 = bf16[1024,512]{1,0:T(8,128)(2,1)} collective-permute-done((bf16[1024,512]{1,0:T(8,128)(2,1)}, bf16[1024,512]{1,0:T(8,128)(2,1)}, u32[]{:S(2)}, u32[]{:S(2)}) %collective-permute-start.6) | collective-permute-done | bytes 1048608 | tf_op jit(solution)/shard_map/ppermute | solution.py:121
  163.1 2.2 add_convert_fusion.2
  165.3 1.8 collective-permute-start.8
  167.1 22.7 %collective-permute-done.8 = bf16[1024,512]{1,0:T(8,128)(2,1)S(1)} collective-permute-done((bf16[1024,512]{1,0:T(8,128)(2,1)S(1)}, bf16[1024,512]{1,0:T(8,128)(2,1)S(1)}, u32[]{:S(2)}, u32[]{:S(2)}) %collective-permute-start.8) | collective-permute-done | bytes 1048608 | tf_op jit(solution)/shard_map/ppermute | solution.py:135
  190.6 1.4 constant_dynamic-update-slice_fusion.2
  192.7 2.0 copy-done.2
  194.8 0.9 fusion
  195.7 12.0 %fusion.12 = f32[1024,1408]{1,0:T(8,128)} fusion(bf16[2048,1408]{1,0:T(8,128)(2,1)} %all-gather.4.cloned.1.call-done, bf16[1024,2048]{1,0:T(8,128)(2,1)} %copy-done.2, f32[2048]{0:T(1024)S(1)} %convert_element_type.90, f32[1024]{0:T(1024)S(1)} %add_rsqrt_fusion), kind=kOutput, calls=%fused_computation.20 | convolution fusion | flops 5913968640 | bytes 15740928 | tf_op jit(solution)/shard_map/dot_general | solution.py:206
  207.6 10.1 %all-gather.6.cloned.1.call-done = bf16[2048,1408]{1,0:T(8,128)(2,1)} async-done(((bf16[256,1408]{1,0:T(8,128)(2,1)}), bf16[2048,1408]{1,0:T(8,128)(2,1)}) %all-gather.6.cloned.1.call-update) | async-done | bytes 5767184 | tf_op jit(solution)/shard_map/all_gather | solution.py:161
  217.8 12.4 %multiply_convert_fusion = bf16[1024,1408]{1,0:T(8,128)(2,1)} fusion(f32[1024,1408]{1,0:T(8,128)} %fusion.12, bf16[2048,1408]{1,0:T(8,128)(2,1)} %all-gather.6.cloned.1.call-done, bf16[1024,2048]{1,0:T(8,128)(2,1)} %copy-done.2, f32[2048]{0:T(1024)S(1)} %convert_element_type.90, f32[1024]{0:T(1024)S(1)} %add_rsqrt_fusion), kind=kOutput, calls=%fused_computation.5 | convolution fusion | flops 5922619392 | bytes 18624512 | tf_op jit(solution)/shard_map/dot_general | solution.py:207
  230.2 80.9 %all-gather.8.cloned.1.call-done = bf16[1408,2048]{1,0:T(8,128)(2,1)} async-done(((bf16[1408,256]{1,0:T(8,128)(2,1)}), bf16[1408,2048]{1,0:T(8,128)(2,1)}) %all-gather.8.cloned.1.call-update) | async-done | bytes 5767184 | tf_op jit(solution)/shard_map/all_gather | solution.py:202
  311.2 4.2 %convolution_convert_fusion = bf16[1024,512]{1,0:T(8,128)(2,1)S(1)} fusion(bf16[1024,1408]{1,0:T(8,128)(2,1)} %multiply_convert_fusion, bf16[1408,2048]{1,0:T(8,128)(2,1)} %all-gather.8.cloned.1.call-done, s32[]{:T(128)S(6)} %select_n.261), kind=kOutput, calls=%fused_computation.10 | convolution fusion | flops 1476919296 | bytes 5373956 | tf_op jit(solution)/shard_map/dot_general | solution.py:111
  316.0 1.8 convolution_convert_fusion.1
  318.0 1.8 add_convert_fusion.1
  319.8 1.5 collective-permute-start.12
  321.4 1.8 fusion.7
  323.2 22.1 %collective-permute-done.12 = bf16[1024,512]{1,0:T(8,128)(2,1)S(1)} collective-permute-done((bf16[1024,512]{1,0:T(8,128)(2,1)S(1)}, bf16[1024,512]{1,0:T(8,128)(2,1)S(1)}, u32[]{:S(2)}, u32[]{:S(2)}) %collective-permute-start.12) | collective-permute-done | bytes 1048608 | tf_op jit(solution)/shard_map/ppermute | solution.py:121
  345.3 1.6 add_convert_fusion
  (87 shorter events, 6.8 us)
Async XLA Ops:
  6.5 120.3 %copy-start = (bf16[512,2048]{1,0:T(8,128)(2,1)S(1)}, bf16[512,2048]{1,0:T(8,128)(2,1)}, u32[]{:S(2)}) copy-start(bf16[512,2048]{1,0:T(8,128)(2,1)} %param.39) | copy-start | bytes 6291460
  6.5 189.1 %all-gather.4.cloned.1.call-start = ((), (), s32[]{:S(2)}) async-start(), calls=%async_computation | async-start | bytes 6488064 | tf_op jit(solution)/shard_map/all_gather | solution.py:160
  7.3 210.5 %all-gather.6.cloned.1.call-start = ((), (), s32[]{:S(2)}) async-start(), calls=%async_computation.1 | async-start | bytes 6488064 | tf_op jit(solution)/shard_map/all_gather | solution.py:161
  8.0 303.1 %all-gather.8.cloned.1.call-start = ((), (), s32[]{:S(2)}) async-start(), calls=%async_computation.2 | async-start | bytes 6488064 | tf_op jit(solution)/shard_map/all_gather | solution.py:202
  13.3 70.3 %copy-start.8 = (bf16[512]{0:T(512)(128)(2,1)S(1)}, bf16[512]{0:T(512)(128)(2,1)}, u32[]{:S(2)}) copy-start(bf16[512]{0:T(512)(128)(2,1)} %param.38) | copy-start | bytes 3076
  16.0 24.3 %collective-permute-start = (f32[2,136,256]{2,1,0:T(8,128)S(1)}, f32[2,136,256]{2,1,0:T(8,128)S(1)}, u32[]{:S(2)}, u32[]{:S(2)}) collective-permute-start(f32[2,136,256]{2,1,0:T(8,128)S(1)} %pad_maximum_fusion), channel_id=1, source_target_pairs={{0,4},{4,8},{8,12},{12,16},{16,20},{20,24},{24,28},{1,5},{5,9},{9,... | collective-permute-start | bytes 835592 | tf_op jit(solution)/shard_map/ppermute | solution.py:31
  40.3 42.4 %copy-start.5 = (f32[2,136,256]{2,1,0:T(8,128)}, f32[2,136,256]{2,1,0:T(8,128)S(1)}, u32[]{:S(2)}) copy-start(f32[2,136,256]{2,1,0:T(8,128)S(1)} %collective-permute-done) | copy-start | bytes 835588
  40.6 15.7 %collective-permute-start.1 = (f32[2,136,256]{2,1,0:T(8,128)S(1)}, f32[2,136,256]{2,1,0:T(8,128)S(1)}, u32[]{:S(2)}, u32[]{:S(2)}) collective-permute-start(f32[2,136,256]{2,1,0:T(8,128)S(1)} %pad_maximum_fusion.1), channel_id=1, source_target_pairs={{0,4},{4,8},{8,12},{12,16},{16,20},{20,24},{24,28},{1,5},{5,9},{9,... | collective-permute-start | bytes 835592 | tf_op jit(solution)/shard_map/ppermute | solution.py:35
  56.3 26.3 %copy-start.6 = (f32[2,136,256]{2,1,0:T(8,128)}, f32[2,136,256]{2,1,0:T(8,128)S(1)}, u32[]{:S(2)}) copy-start(f32[2,136,256]{2,1,0:T(8,128)S(1)} %collective-permute-done.1) | copy-start | bytes 835588
  56.8 20.8 %collective-permute-start.2 = (f32[2,136,256]{2,1,0:T(8,128)S(1)}, f32[2,136,256]{2,1,0:T(8,128)}, u32[]{:S(2)}, u32[]{:S(2)}) collective-permute-start(f32[2,136,256]{2,1,0:T(8,128)S(1)} %pad_maximum_fusion.2), channel_id=1, source_target_pairs={{0,8},{4,12},{8,16},{12,20},{16,24},{20,28},{1,9},{5,13},{9,17},{1... | collective-permute-start | bytes 835592 | tf_op jit(solution)/shard_map/ppermute | solution.py:35
  80.5 32.9 %collective-permute-start.3 = (f32[2,136,256]{2,1,0:T(8,128)}, f32[2,136,256]{2,1,0:T(8,128)}, u32[]{:S(2)}, u32[]{:S(2)}) collective-permute-start(f32[2,136,256]{2,1,0:T(8,128)} %pad_maximum_fusion.3), channel_id=1, source_target_pairs={{0,16},{4,20},{8,24},{12,28},{1,17},{5,21},{9,25},{13,29},{2,18},{... | collective-permute-start | bytes 835592 | tf_op jit(solution)/shard_map/ppermute | solution.py:35
  126.8 6.5 %copy-start.3 = (bf16[1024,512]{1,0:T(8,128)(2,1)S(1)}, bf16[1024,512]{1,0:T(8,128)(2,1)}, u32[]{:S(2)}) copy-start(bf16[1024,512]{1,0:T(8,128)(2,1)} %cell.1) | copy-start | bytes 3145732
  129.8 3.5 collective-permute-start.5
  132.8 7.3 %collective-permute-start.4 = (bf16[1024,512]{1,0:T(8,128)(2,1)}, bf16[1024,512]{1,0:T(8,128)(2,1)}, u32[]{:S(2)}, u32[]{:S(2)}) collective-permute-start(bf16[1024,512]{1,0:T(8,128)(2,1)} %convolution_convert_fusion.3), channel_id=1, source_target_pairs={{0,1},{1,0},{2,3},{3,2},{4,5},{5,4},{6,7},{7,6},{8,9},{9,8},{10,11... | collective-permute-start | bytes 3145736 | tf_op jit(solution)/shard_map/ppermute | solution.py:115
  136.3 26.8 %collective-permute-start.6 = (bf16[1024,512]{1,0:T(8,128)(2,1)}, bf16[1024,512]{1,0:T(8,128)(2,1)}, u32[]{:S(2)}, u32[]{:S(2)}) collective-permute-start(bf16[1024,512]{1,0:T(8,128)(2,1)} %add_convert_fusion.3), channel_id=1, source_target_pairs={{0,2},{1,3},{2,0},{3,1},{4,6},{5,7},{6,4},{7,5},{8,10},{9,11},{10,... | collective-permute-start | bytes 3145736 | tf_op jit(solution)/shard_map/ppermute | solution.py:121
  139.4 23.6 %copy-start.4 = (bf16[1024,512]{1,0:T(8,128)(2,1)S(1)}, bf16[1024,512]{1,0:T(8,128)(2,1)}, u32[]{:S(2)}) copy-start(bf16[1024,512]{1,0:T(8,128)(2,1)} %param.37) | copy-start | bytes 3145732
  140.1 49.7 %copy-start.7 = (bf16[2048]{0:T(1024)(128)(2,1)S(1)}, bf16[2048]{0:T(1024)(128)(2,1)}, u32[]{:S(2)}) copy-start(bf16[2048]{0:T(1024)(128)(2,1)} %param.40) | copy-start | bytes 12292
  165.3 24.6 %collective-permute-start.8 = (bf16[1024,512]{1,0:T(8,128)(2,1)S(1)}, bf16[1024,512]{1,0:T(8,128)(2,1)S(1)}, u32[]{:S(2)}, u32[]{:S(2)}) collective-permute-start(bf16[1024,512]{1,0:T(8,128)(2,1)S(1)} %add_convert_fusion.2), channel_id=1, source_target_pairs={{0,2},{1,3},{2,0},{3,1},{4,6},{5,7},{6,4},{7,5},{8,10},{9,11},{10,... | collective-permute-start | bytes 3145736 | tf_op jit(solution)/shard_map/ppermute | solution.py:135
  167.1 23.5 %collective-permute-start.7 = (bf16[1024,512]{1,0:T(8,128)(2,1)S(1)}, bf16[1024,512]{1,0:T(8,128)(2,1)}, u32[]{:S(2)}, u32[]{:S(2)}) collective-permute-start(bf16[1024,512]{1,0:T(8,128)(2,1)S(1)} %add_convert_fusion.2), channel_id=1, source_target_pairs={{0,1},{1,0},{2,3},{3,2},{4,5},{5,4},{6,7},{7,6},{8,9},{9,8},{10,11... | collective-permute-start | bytes 3145736 | tf_op jit(solution)/shard_map/ppermute | solution.py:138
  189.9 2.7 collective-permute-start.9
  192.7 2.0 copy-start.2
  311.2 4.2 %copy-start.9 = (bf16[1408,2048]{1,0:T(8,128)(2,1)S(1)}, bf16[1408,2048]{1,0:T(8,128)(2,1)}, u32[]{:S(2)}) copy-start(bf16[1408,2048]{1,0:T(8,128)(2,1)} %all-gather.8.cloned.1.call-done) | copy-start | bytes 17301508
  311.2 4.8 %copy-start.10 = (bf16[1024,1408]{1,0:T(8,128)(2,1)S(1)}, bf16[1024,1408]{1,0:T(8,128)(2,1)}, u32[]{:S(2)}) copy-start(bf16[1024,1408]{1,0:T(8,128)(2,1)} %multiply_convert_fusion) | copy-start | bytes 8650756
  315.3 2.7 collective-permute-start.11
  317.8 5.4 %collective-permute-start.10 = (bf16[1024,512]{1,0:T(8,128)(2,1)S(1)}, bf16[1024,512]{1,0:T(8,128)(2,1)S(1)}, u32[]{:S(2)}, u32[]{:S(2)}) collective-permute-start(bf16[1024,512]{1,0:T(8,128)(2,1)S(1)} %convolution_convert_fusion.1), channel_id=1, source_target_pairs={{0,1},{1,0},{2,3},{3,2},{4,5},{5,4},{6,7},{7,6},{8,9},{9,8},{10,11... | collective-permute-start | bytes 3145736 | tf_op jit(solution)/shard_map/ppermute | solution.py:115
  319.8 25.5 %collective-permute-start.12 = (bf16[1024,512]{1,0:T(8,128)(2,1)S(1)}, bf16[1024,512]{1,0:T(8,128)(2,1)S(1)}, u32[]{:S(2)}, u32[]{:S(2)}) collective-permute-start(bf16[1024,512]{1,0:T(8,128)(2,1)S(1)} %add_convert_fusion.1), channel_id=1, source_target_pairs={{0,2},{1,3},{2,0},{3,1},{4,6},{5,7},{6,4},{7,5},{8,10},{9,11},{10,... | collective-permute-start | bytes 3145736 | tf_op jit(solution)/shard_map/ppermute | solution.py:121
  321.4 25.6 %copy-start.1 = (bf16[512,2048]{1,0:T(8,128)(2,1)S(1)}, bf16[512,2048]{1,0:T(8,128)(2,1)}, u32[]{:S(2)}) copy-start(bf16[512,2048]{1,0:T(8,128)(2,1)} %param.39) | copy-start | bytes 6291460
Sparse Core Ops, SparseCore 0:
  9.5 114.5 all-gather.3
  126.3 91.4 all-gather.5
  219.8 91.2 all-gather.7
where the time goes:
time: 358 us; the launch traced here: 353 us
  waiting for transfers between devices  244 us (68%)
  matrix products  46.1 us (13%)
  other arithmetic  15.8 us (4%)
  starting transfers between devices  15.3 us (4%)
  between operations  13.5 us (4%)
  local copies, waits for them, and re-layouts  9.38 us (3%)
  Pallas kernels  9.13 us (3%)
    all_gather x1, waiting for transfers between devices, local(): whole_down = lax.all_gather(down_late, 'sp', axis=1, tiled=True)  80.9 us
    ppermute x3, waiting for transfers between devices, entering_state(): moved = lax.ppermute(pack(s, t, f), 'sp', shift_pairs(length, step))  62.6 us
    ppermute x2, waiting for transfers between devices, product_scattered(): moved.append(lax.ppermute(sent, 'tp', ring_pairs(count, step)))  45 us
    ppermute x1, waiting for transfers between devices, columns_gathered(): moved = lax.ppermute(block, 'tp', ring_pairs(count, step))  22.7 us
    ppermute x1, waiting for transfers between devices, entering_state(): moved = lax.ppermute(pack(state, top, total), 'sp', shift_pairs(length, 1))  20.8 us
    dot_general x8, matrix products, product(): return jnp.dot(rows, columns, preferred_element_type=jnp.float32)  19.1 us
    dot_general x1, matrix products, local(): lifted = jnp.dot(normed, whole_up, preferred_element_type=jnp.float32)  12.4 us
    dot_general x1, matrix products, local(): gate_value = jnp.dot(normed, whole_gate, preferred_element_type=jnp.float32)  12 us
  transfers between devices with their start and end apart: 16, of which 11 were waited for; matrix products, arithmetic and copies ran while one was open for 18% of the time, Pallas kernels for 3%

commit v1 on v0

--- a/solution.py
+++ b/solution.py
@@ -1,3 +1,5 @@
+import functools
+
 import jax
 import jax.numpy as jnp
 from jax import lax
@@ -141,7 +143,7 @@
     return whole
 
 
-def local(
+def general(
     queries,
     cell_key_rows,
     cell_value_rows,
@@ -210,6 +212,708 @@
     return (stream.astype(jnp.float32) + 0.5 * channel_total).astype(jnp.bfloat16)
 
 
+NX, NY = 2, 2
+BY_NAME = pl.DeviceIdType.MESH
+
+
+def block_body(
+    planes,
+    q_ref,
+    k_ref,
+    v_ref,
+    open_ref,
+    a_ref,
+    cols_ref,
+    meta_ref,
+    resid_ref,
+    gain_ref,
+    wo_ref,
+    fgain_ref,
+    gate_ref,
+    up_ref,
+    down_ref,
+    out_ref,
+    gu,
+    dn,
+    rows_all,
+    hid,
+    gu_out,
+    num,
+    ent,
+    st_own,
+    st_y,
+    st_sum,
+    st_z,
+    meta_y,
+    meta_sum,
+    meta_z,
+    lw_ref,
+    pool,
+    core_in,
+    x_in,
+    normed,
+    core_back,
+    y_back,
+    x_back,
+    zs,
+    zr,
+    ysem,
+    ssem,
+    fsem,
+    gsem,
+    bsem,
+    lsem,
+):
+    sp, tp = lax.axis_index("sp"), lax.axis_index("tp")
+    z, y, x, c = sp // NY, sp % NY, tp // 2, tp % 2
+    tokens, heads = q_ref.shape[0], a_ref.shape[0]
+    dk, dv = q_ref.shape[1] // heads, v_ref.shape[1] // heads
+    width = resid_ref.shape[1]
+    depth, hidden = gate_ref.shape
+    half = hidden // NY
+    count = 2 * NX
+    last = planes - 1
+    strip = tokens // 4
+    wide = width // 2
+    part_rows = depth // 2
+
+    partner = {"tp": tp + 1 - 2 * c}
+    x_next = {"tp": (1 - x) * 2 + c}
+    y_next = {"sp": z * NY + 1 - y}
+
+    def on_plane(at):
+        return {"sp": at * NY + y}
+
+    def remote(src, dst, sems, to):
+        return pltpu.make_async_remote_copy(
+            src_ref=src, dst_ref=dst, send_sem=sems[0], recv_sem=sems[1], device_id=to, device_id_type=BY_NAME
+        )
+
+    barrier = pltpu.get_barrier_semaphore()
+    for to in (partner, x_next, y_next):
+        pl.semaphore_signal(barrier, inc=1, device_id=to, device_id_type=BY_NAME)
+    for step in range(1, planes):
+        pl.semaphore_signal(
+            barrier, inc=1, device_id=on_plane((z + step) % planes), device_id_type=BY_NAME
+        )
+    pl.semaphore_wait(barrier, planes + 2)
+
+    for mine in range(NY):
+
+        @pl.when(y == mine)
+        def _():
+            own = pl.ds(pl.multiple_of(sp * depth, depth), depth)
+            here, there = mine * half, (1 - mine) * half
+            gu_out[:, 0:half] = gate_ref[:, there : there + half]
+            gu_out[:, half : 2 * half] = up_ref[:, there : there + half]
+            gu[own, 0:half] = gate_ref[:, here : here + half]
+            gu[own, half : 2 * half] = up_ref[:, here : here + half]
+
+    def gu_rows(at, chunk):
+        side = (y + chunk // 2) % 2
+        start = (at * NY + side) * depth + (chunk % 2) * part_rows
+        return pl.ds(pl.multiple_of(start, part_rows), part_rows)
+
+    def z_copy(way, dist, chunk):
+        at = z - dist if way == 0 else z + dist
+        to = z + 1 if way == 0 else z - 1
+        sems = (zs.at[way, dist, chunk], zr.at[way, dist + 1, chunk])
+        if chunk < 4:
+            part = gu.at[gu_rows(at, chunk), :]
+        else:
+            part = dn.at[at * NY + chunk - 4]
+        return remote(part, part, sems, on_plane(to))
+
+    def z_arrival(way, dist, chunk):
+        at = z - dist if way == 0 else z + dist
+        sems = (zs.at[way, dist, chunk], zr.at[way, dist, chunk])
+        if chunk < 4:
+            part = gu.at[gu_rows(at, chunk), :]
+        else:
+            part = dn.at[at * NY + chunk - 4]
+        return remote(part, part, sems, on_plane(z))
+
+    def has_next(way):
+        return z < last if way == 0 else z > 0
+
+    def has_origin(way, dist):
+        return z >= dist if way == 0 else z + dist <= last
+
+    def z_send(chunk):
+        for way in range(2):
+
+            @pl.when(has_next(way))
+            def _():
+                z_copy(way, 0, chunk).start()
+
+    def z_forward(dist, chunk):
+        for way in range(2):
+
+            @pl.when(jnp.logical_and(has_origin(way, dist), has_next(way)))
+            def _():
+                z_arrival(way, dist, chunk).wait_recv()
+                z_copy(way, dist, chunk).start()
+
+    def y_rows(owner, chunk):
+        start = (z * NY + owner) * depth + chunk * part_rows
+        return pl.ds(pl.multiple_of(start, part_rows), part_rows)
+
+    def y_weight(chunk):
+        sems = (ysem.at[0, chunk], ysem.at[1, chunk])
+        if chunk < 2:
+            return remote(
+                gu_out.at[pl.ds(chunk * part_rows, part_rows), :], gu.at[y_rows(y, chunk), :], sems, y_next
+            )
+        start = pl.multiple_of((1 - y) * half, half)
+        return remote(down_ref.at[pl.ds(start, half), :], dn.at[sp], sems, y_next)
+
+    own_down = pltpu.make_async_copy(
+        down_ref.at[pl.ds(pl.multiple_of(y * half, half), half), :], dn.at[sp], lsem.at[0]
+    )
+    own_down.start()
+    y_weight(0).start()
+    z_send(0)
+
+    for h in range(heads):
+        weighed = (
+            k_ref[:, h * dk : (h + 1) * dk].astype(jnp.float32) * cols_ref[:, h : h + 1]
+        ).astype(jnp.bfloat16)
+        st_own[h] = lax.dot_general(
+            weighed,
+            v_ref[:, h * dv : (h + 1) * dv],
+            (((0,), (0,)), ((), ())),
+            preferred_element_type=jnp.float32,
+        ).astype(jnp.bfloat16)
+
+    state_y = [
+        remote(st_own, st_y, (ssem.at[0, 0], ssem.at[0, 1]), y_next),
+        remote(meta_ref, meta_y, (ssem.at[1, 0], ssem.at[1, 1]), y_next),
+    ]
+    for copy in state_y:
+        copy.start()
+    y_weight(1).start()
+    y_weight(2).start()
+    z_send(1)
+
+    def attend(h, i):
+        span = (i + 1) * strip
+        at = pl.ds(i * strip, strip)
+        scores = lax.dot_general(
+            q_ref[at, h * dk : (h + 1) * dk],
+            k_ref[0:span, h * dk : (h + 1) * dk],
+            (((1,), (1,)), ((), ())),
+            preferred_element_type=jnp.float32,
+        )
+        log_weight = a_ref[h : h + 1, 0:span] - cols_ref[at, heads + h : heads + h + 1]
+        row = i * strip + lax.broadcasted_iota(jnp.int32, (strip, span), 0)
+        col = lax.broadcasted_iota(jnp.int32, (strip, span), 1)
+        weight = jnp.where(col <= row, jnp.exp(jnp.minimum(log_weight, 0.0)), 0.0)
+        num[at, h * dv : (h + 1) * dv] = jnp.dot(
+            (scores * weight).astype(jnp.bfloat16),
+            v_ref[0:span, h * dv : (h + 1) * dv],
+            preferred_element_type=jnp.float32,
+        )
+
+    for h in range(heads):
+        attend(h, 0)
+
+    for copy in state_y:
+        copy.wait_recv()
+    first = y == 0
+    meta_own, meta_other = meta_ref[...], meta_y[...]
+    meta_0 = jnp.where(first, meta_own, meta_other)
+    meta_1 = jnp.where(first, meta_other, meta_own)
+    top_0 = meta_0[0:heads] + meta_1[heads : 2 * heads]
+    top_1 = meta_1[0:heads]
+    top = jnp.maximum(top_0, top_1)
+    scale_0, scale_1 = jnp.exp(top_0 - top), jnp.exp(top_1 - top)
+    scale_own = jnp.where(first, scale_0, scale_1)
+    scale_other = jnp.where(first, scale_1, scale_0)
+    meta_sum[...] = jnp.zeros_like(meta_sum)
+    meta_sum[0:heads, :] = top
+    meta_sum[heads : 2 * heads, :] = meta_0[heads : 2 * heads] + meta_1[heads : 2 * heads]
+    for h in range(heads):
+        st_sum[h] = (
+            st_own[h].astype(jnp.float32) * scale_own[h : h + 1]
+            + st_y[h].astype(jnp.float32) * scale_other[h : h + 1]
+        ).astype(jnp.bfloat16)
+
+    def state_z(step, source):
+        kept = st_z.at[source], meta_z.at[source]
+        to = on_plane(z + step)
+        return [
+            remote(st_sum, kept[0], (ssem.at[2, step], ssem.at[3, source]), to),
+            remote(meta_sum, kept[1], (ssem.at[4, step], ssem.at[5, source]), to),
+        ]
+
+    for step in range(1, planes):
+
+        @pl.when(z + step <= last)
+        def _():
+            for copy in state_z(step, z):
+                copy.start()
+
+    for chunk in range(2):
+        y_weight(chunk).wait_recv()
+        z_send(2 + chunk)
+
+    for h in range(heads):
+        for i in range(1, 4):
+            attend(h, i)
+
+    low = jnp.full((heads, meta_ref.shape[1]), LOWEST_LOG, jnp.float32)
+    later = jnp.where(y == 1, meta_y[heads : 2 * heads, :], 0.0)
+    lw_ref[planes - 1, 0:heads, :] = jnp.where(y == 1, meta_y[0:heads, :], low)
+    ctop = lw_ref[planes - 1, 0:heads, :]
+    for source in range(planes - 2, -1, -1):
+        valid = z > source
+
+        @pl.when(valid)
+        def _():
+            for copy in state_z(0, source):
+                copy.wait_recv()
+
+        here = jnp.where(valid, meta_z[source, 0:heads, :] + later, low)
+        lw_ref[source, 0:heads, :] = here
+        ctop = jnp.maximum(ctop, here)
+        later = later + jnp.where(valid, meta_z[source, heads : 2 * heads, :], 0.0)
+    ent[...] = jnp.zeros_like(ent)
+    for source in range(planes):
+        valid = z > source if source < planes - 1 else y == 1
+
+        @pl.when(valid)
+        def _():
+            scale = jnp.exp(lw_ref[source, 0:heads, :] - ctop)
+            for h in range(heads):
+                part = st_z[source, h] if source < planes - 1 else st_y[h]
+                ent[h] += part.astype(jnp.float32) * scale[h : h + 1]
+
+    z_forward(1, 0)
+    z_forward(1, 1)
+    z_forward(1, 2)
+
+    def front_core(i):
+        at = pl.ds(pl.multiple_of(i * strip, strip), strip)
+        return remote(
+            pool.at[0:4, at, :], core_in.at[:, at, :], (fsem.at[0, i], fsem.at[1, i]), partner
+        )
+
+    def front_x(i):
+        at = pl.ds(pl.multiple_of(i * strip, strip), strip)
+        return remote(
+            pool.at[8:10, at, :], x_in.at[:, at, :], (fsem.at[2, i], fsem.at[3, i]), x_next
+        )
+
+    def gate_strip(i):
+        at = pl.ds(pl.multiple_of(i * strip, strip), strip)
+        gated = []
+        for h in range(heads):
+            lanes = slice(h * dv, (h + 1) * dv)
+            before = jnp.dot(
+                q_ref[at, h * dk : (h + 1) * dk],
+                ent[h].astype(jnp.bfloat16),
+                preferred_element_type=jnp.float32,
+            )
+            m_log = cols_ref[at, heads + h : heads + h + 1]
+            m_all = jnp.maximum(m_log, ctop[h : h + 1, 0:1])
+            memory = (
+                num[at, lanes] * jnp.exp(m_log - m_all)
+                + jnp.exp(ctop[h : h + 1, 0:1] - m_all) * before
+            ) * dk ** (-0.5)
+            normal = memory * lax.rsqrt(jnp.mean(memory * memory, axis=-1, keepdims=True) + EPSILON)
+            opened = jax.nn.sigmoid(open_ref[at, lanes].astype(jnp.float32))
+            gated.append((normal * gain_ref[0:1, lanes].astype(jnp.float32) * opened).astype(jnp.bfloat16))
+        gated = jnp.concatenate(gated, axis=1)
+        for chip in range(NX):
+            for part in range(2):
+                for mine in range(2):
+                    core = c if mine else 1 - c
+                    lanes = pl.ds(
+                        pl.multiple_of((chip * 2 + core) * width + part * wide, wide), wide
+                    )
+                    pool[mine * 4 + chip * 2 + part, at, :] = jnp.dot(
+                        gated, wo_ref[:, lanes], preferred_element_type=jnp.float32
+                    ).astype(jnp.bfloat16)
+        front_core(i).start()
+
+    def core_sum(i):
+        at = pl.ds(pl.multiple_of(i * strip, strip), strip)
+        front_core(i).wait_recv()
+        for part in range(2):
+            far, near = (1 - x) * 2 + part, x * 2 + part
+            pool[8 + part, at, :] = (
+                pool[4 + far, at, :].astype(jnp.float32) + core_in[far, at, :].astype(jnp.float32)
+            ).astype(jnp.bfloat16)
+        front_x(i).start()
+
+    @pl.loop(0, 5)
+    def _(i):
+        @pl.when(i < 4)
+        def _():
+            gate_strip(i)
+
+        @pl.when(i >= 1)
+        def _():
+            core_sum(i - 1)
+
+    z_forward(1, 3)
+    z_forward(2, 0)
+    y_weight(2).wait_recv()
+    own_down.wait()
+
+    def piece(owner_x, owner_c, owner_y, i):
+        at = pl.multiple_of(owner_y * tokens + i * strip, strip)
+        return rows_all.at[owner_x * 2 + owner_c, pl.ds(at, strip), :]
+
+    def to_x(i):
+        part = piece(x, c, y, i)
+        return remote(part, part, (gsem.at[0, i], gsem.at[1, i]), x_next)
+
+    def to_y(kind, i):
+        part = piece(x if kind == 0 else 1 - x, c, y, i)
+        return remote(part, part, (gsem.at[2 + kind, i], gsem.at[4 + kind, i]), y_next)
+
+    def to_core(kind, i):
+        part = piece(
+            x if kind % 2 == 0 else 1 - x, c, y if kind // 2 == 0 else 1 - y, i
+        )
+        return remote(part, part, (gsem.at[6 + kind, i], gsem.at[10 + kind, i]), partner)
+
+    @pl.loop(0, 4)
+    def _(i):
+        at = pl.ds(pl.multiple_of(i * strip, strip), strip)
+        front_x(i).wait_recv()
+        start = pl.multiple_of(y * tokens + i * strip, strip)
+        for part in range(2):
+            lanes = slice(part * wide, (part + 1) * wide)
+            near = x * 2 + part
+            total = (
+                pool[4 + near, at, :].astype(jnp.float32)
+                + core_in[near, at, :].astype(jnp.float32)
+                + x_in[part, at, :].astype(jnp.float32)
+            )
+            rows_all[tp, pl.ds(start, strip), lanes] = (
+                resid_ref[at, lanes].astype(jnp.float32) + total
+            ).astype(jnp.bfloat16)
+        to_x(i).start()
+        to_y(0, i).start()
+        to_core(0, i).start()
+
+    z_forward(2, 1)
+
+    @pl.loop(0, 4)
+    def _(i):
+        to_x(i).wait_recv()
+        to_y(1, i).start()
+        to_core(1, i).start()
+
+    z_forward(2, 2)
+    z_forward(2, 3)
+    z_send(4)
+    z_send(5)
+
+    @pl.loop(0, 4)
+    def _(i):
+        to_y(0, i).wait_recv()
+        to_core(2, i).start()
+
+    @pl.loop(0, 4)
+    def _(i):
+        to_y(1, i).wait_recv()
+        to_core(3, i).start()
+
+    for dist in range(1, planes - 1):
+        for chunk in (4, 5):
+            z_forward(dist, chunk)
+
+    for way in range(2):
+        for dist in range(1, planes):
+
+            @pl.when(jnp.logical_and(has_origin(way, dist), jnp.logical_not(has_next(way))))
+            def _():
+                for chunk in range(4):
+                    z_arrival(way, dist, chunk).wait_recv()
+
+    @pl.loop(0, 4)
+    def _(i):
+        for kind in range(4):
+            to_core(kind, i).wait_recv()
+
+    @pl.loop(0, 4)
+    def _(i):
+        for copy in (front_core(i), front_x(i), to_x(i), to_y(0, i), to_y(1, i)):
+            copy.wait_send()
+        for kind in range(4):
+            to_core(kind, i).wait_send()
+
+    tall = normed.shape[0]
+
+    @pl.loop(0, NY * tokens // tall)
+    def _(i):
+        base = pl.multiple_of(i * tall, tall)
+
+        @pl.loop(0, tall // 64)
+        def _(r):
+            at = pl.ds(pl.multiple_of(base + r * 64, 64), 64)
+            parts = [rows_all[j, at, :].astype(jnp.float32) for j in range(count)]
+            square = sum(jnp.sum(p * p, axis=-1, keepdims=True) for p in parts)
+            scale = lax.rsqrt(square / (count * width) + EPSILON)
+            to = pl.ds(pl.multiple_of(r * 64, 64), 64)
+            for j in range(count):
+                lanes = slice(j * width, (j + 1) * width)
+                normed[to, lanes] = (parts[j] * scale * fgain_ref[0:1, lanes].astype(jnp.float32)).astype(
+                    jnp.bfloat16
+                )
+
+        both = jnp.dot(normed[...], gu[...], preferred_element_type=jnp.float32)
+        hid[pl.ds(base, tall), :] = (jax.nn.silu(both[:, :half]) * both[:, half:]).astype(jnp.bfloat16)
+
+    units = planes * NY
+
+    def place(unit):
+        step = unit // NY
+        low_bit = (z % 2 + step % 2) % 2
+        high = (z // 2 + step // 2) % 2
+        return high * 2 + low_bit
+
+    def slot(unit):
+        return unit // 4 * 2 + unit % 2
+
+    def back_core(unit):
+        return remote(
+            pool.at[pl.ds(unit * 2, 2)], core_back.at[slot(unit)], (bsem.at[0, unit], bsem.at[1, unit]), partner
+        )
+
+    def back_y(unit):
+        return remote(
+            pool.at[unit * 2 + 1 - y], y_back.at[slot(unit)], (bsem.at[2, unit], bsem.at[3, unit]), y_next
+        )
+
+    def back_x(unit):
+        return remote(
+            pool.at[unit * 2 + y], x_back.at[unit % 2], (bsem.at[4, unit], bsem.at[5, unit]), x_next
+        )
+
+    def keeps(unit):
+        return place(unit) % 2 == c
+
+    def owns(unit):
+        return place(unit) == tp
+
+    def passes(unit):
+        return jnp.logical_and(keeps(unit), place(unit) // 2 != x)
+
+    def down_part(unit):
+        step, side = unit // NY, unit % NY
+
+        @pl.when(jnp.logical_and(step > 0, jnp.logical_or(z == 0, z == last)))
+        def _():
+            at = place(unit) * NY + side
+            way = jnp.where(z == 0, 1, 0)
+            part = dn.at[at]
+            remote(part, part, (zs.at[way, step, 4 + side], zr.at[way, step, 4 + side]), on_plane(z)).wait_recv()
+
+        weight = dn[place(unit) * NY + side]
+        for top_row in range(NY):
+            for quarter in range(2):
+                rows = tokens // 2
+                start = top_row * tokens + quarter * rows
+                pool[unit * 2 + top_row, pl.ds(quarter * rows, rows), :] = jnp.dot(
+                    hid[pl.ds(start, rows), :], weight, preferred_element_type=jnp.float32
+                ).astype(jnp.bfloat16)
+
+        @pl.when(jnp.logical_not(keeps(unit)))
+        def _():
+            back_core(unit).start()
+
+    def after_core(unit):
+        @pl.when(keeps(unit))
+        def _():
+            back_core(unit).wait_recv()
+            for side in (1 - y, y):
+                pool[unit * 2 + side] = (
+                    pool[unit * 2 + side].astype(jnp.float32)
+                    + core_back[slot(unit), side].astype(jnp.float32)
+                ).astype(jnp.bfloat16)
+            back_y(unit).start()
+
+    def after_y(unit):
+        @pl.when(keeps(unit))
+        def _():
+            back_y(unit).wait_recv()
+            pool[unit * 2 + y] = (
+                pool[unit * 2 + y].astype(jnp.float32) + y_back[slot(unit)].astype(jnp.float32)
+            ).astype(jnp.bfloat16)
+
+        @pl.when(passes(unit))
+        def _():
+            back_x(unit).start()
+
+    def after_x(unit):
+        @pl.when(owns(unit))
+        def _():
+            back_x(unit).wait_recv()
+            total = pool[unit * 2 + y].astype(jnp.float32) + x_back[unit % 2].astype(jnp.float32)
+            lanes = pl.ds(pl.multiple_of((unit % 2) * wide, wide), wide)
+            mine = pl.ds(pl.multiple_of(y * tokens, tokens), tokens)
+            out_ref[:, lanes] = (
+                rows_all[tp, mine, lanes].astype(jnp.float32) + 0.5 * total
+            ).astype(out_ref.dtype)
+
+    @pl.loop(0, units + 3)
+    def _(i):
+        @pl.when(i < units)
+        def _():
+            down_part(i)
+
+        @pl.when(jnp.logical_and(i >= 1, i < units + 1))
+        def _():
+            after_core(i - 1)
+
+        @pl.when(jnp.logical_and(i >= 2, i < units + 2))
+        def _():
+            after_y(i - 2)
+
+        @pl.when(i >= 3)
+        def _():
+            after_x(i - 3)
+
+    @pl.loop(0, units)
+    def _(i):
+        @pl.when(jnp.logical_not(keeps(i)))
+        def _():
+            back_core(i).wait_send()
+
+        @pl.when(keeps(i))
+        def _():
+            back_y(i).wait_send()
+
+        @pl.when(passes(i))
+        def _():
+            back_x(i).wait_send()
+
+    for chunk in range(3):
+        y_weight(chunk).wait_send()
+    for copy in state_y:
+        copy.wait_send()
+    for step in range(1, planes):
+
+        @pl.when(z + step <= last)
+        def _():
+            for copy in state_z(step, z):
+                copy.wait_send()
+
+    for way in range(2):
+        for dist in range(planes - 1):
+
+            @pl.when(jnp.logical_and(has_origin(way, dist), has_next(way)))
+            def _():
+                for chunk in range(6):
+                    z_copy(way, dist, chunk).wait_send()
+
+
+def plane_layer(
+    planes,
+    queries,
+    cell_key_rows,
+    cell_value_rows,
+    output_gate_logits,
+    input_gate_logits,
+    forget_gate_logits,
+    forget_extra_term,
+    residual,
+    head_norm_gain,
+    cell_output_weight,
+    feedforward_norm_gain,
+    gate_projection_weight,
+    up_projection_weight,
+    down_projection_weight,
+):
+    tokens, heads = queries.shape[0], input_gate_logits.shape[0]
+    width = residual.shape[1]
+    model = cell_output_weight.shape[1]
+    depth, hidden = gate_projection_weight.shape
+    half = hidden // NY
+    dk, dv = queries.shape[1] // heads, cell_value_rows.shape[1] // heads
+    log_forget = jax.nn.log_sigmoid(forget_gate_logits.astype(jnp.float32)) + forget_extra_term
+    running = jnp.cumsum(log_forget, axis=-1)
+    a_log = input_gate_logits.astype(jnp.float32) - running
+    m_log = lax.cummax(a_log, axis=1)
+    a_top, total = m_log[:, -1], running[:, -1]
+    decay = jnp.exp(a_log - a_top[:, None])
+    cols = jnp.concatenate([decay, m_log], axis=0).T
+    meta = jnp.concatenate([a_top + total, total, jnp.zeros((8 - 2 * heads,), jnp.float32)])
+    meta = jnp.broadcast_to(meta[:, None], (8, dv))
+    bf16, f32 = jnp.bfloat16, jnp.float32
+    vmem, dma = pltpu.VMEM, pltpu.SemaphoreType.DMA
+    scratch = [
+        vmem((model, hidden), bf16),
+        vmem((planes * NY, half, depth), bf16),
+        vmem((2 * NX, NY * tokens, width), bf16),
+        vmem((NY * tokens, half), bf16),
+        vmem((depth, hidden), bf16),
+        vmem((tokens, heads * dv), f32),
+        vmem((heads, dk, dv), f32),
+        vmem((heads, dk, dv), bf16),
+        vmem((heads, dk, dv), bf16),
+        vmem((heads, dk, dv), bf16),
+        vmem((planes - 1, heads, dk, dv), bf16),
+        vmem((8, dv), f32),
+        vmem((8, dv), f32),
+        vmem((planes - 1, 8, dv), f32),
+        vmem((planes, 8, dv), f32),
+        vmem((2 * planes * NY, tokens, width // 2), bf16),
+        vmem((4, tokens, width // 2), bf16),
+        vmem((2, tokens, width // 2), bf16),
+        vmem((512, model), bf16),
+        vmem((planes * NY // 2, 2, tokens, width // 2), bf16),
+        vmem((planes * NY // 2, tokens, width // 2), bf16),
+        vmem((2, tokens, width // 2), bf16),
+        dma((2, planes, 6)),
+        dma((2, planes, 6)),
+        dma((2, 3)),
+        dma((6, planes)),
+        dma((4, 4)),
+        dma((14, 4)),
+        dma((6, planes * NY)),
+        dma((1,)),
+    ]
+    whole = pl.BlockSpec(memory_space=pltpu.VMEM)
+    return pl.pallas_call(
+        functools.partial(block_body, planes),
+        out_shape=jax.ShapeDtypeStruct((tokens, width), bf16),
+        in_specs=[whole] * 14,
+        out_specs=whole,
+        scratch_shapes=scratch,
+        compiler_params=pltpu.CompilerParams(
+            collective_id=0, has_side_effects=True, vmem_limit_bytes=67043328
+        ),
+        cost_estimate=pl.CostEstimate(flops=22 * 10**9, bytes_accessed=10**7, transcendentals=0),
+        name="block",
+    )(
+        queries,
+        cell_key_rows,
+        cell_value_rows,
+        output_gate_logits,
+        a_log,
+        cols,
+        meta,
+        residual,
+        head_norm_gain[None, :],
+        cell_output_weight,
+        feedforward_norm_gain[None, :],
+        gate_projection_weight,
+        up_projection_weight,
+        down_projection_weight,
+    )
+
+
+def layer(rows, columns, *arrays):
+    if columns == 2 * NX and rows == 4 * NY:
+        return plane_layer(rows // NY, *arrays)
+    return general(*arrays)
+
+
 def solution(mesh):
     placed = (
         P("sp", "tp"),
@@ -228,5 +932,5 @@
         P("tp", "sp"),
     )
     return jax.shard_map(
-        local, mesh=mesh, in_specs=placed, out_specs=P("sp", "tp"), check_vma=False
+        functools.partial(layer, mesh.shape["sp"], mesh.shape["tp"]), mesh=mesh, in_specs=placed, out_specs=P("sp", "tp"), check_vma=False
     )

time: 358 us -> 238 us (0.66)
  the two profiles are of different devices: /device:TPU:24 before, /device:TPU:10 now
where the time goes in v1:
time: 238 us; the launch traced here: 237 us
  Pallas kernels  227 us (95%)
  local copies, waits for them, and re-layouts  7.06 us (3%)
  other arithmetic  3.29 us (1%)
    pallas_call x1, Pallas kernels, plane_layer(): pl.pallas_call(functools.partial(block_body, planes), out_shape=jax.Shape...  227 us

profile of v1, /device:TPU:10, one launch (start us, length us, event | category | flops | bytes accessed | tf_op | source)
XLA Modules:
  0.0 237.3 jit_solution(5532013011259869127)
XLA Ops:
  0.0 1.3 broadcast_in_dim.13.gain_ref
  1.3 0.7 fusion.2
  2.0 0.6 reduce-window.14
  2.6 0.2 slice_reduce_fusion.1
  2.7 0.2 reduce-window.15
  2.9 0.1 add_bitcast_fusion
  3.0 0.7 convert_subtract_fusion.a_ref
  3.7 0.0 copy-start
  3.7 0.6 reduce-window.16
  4.3 0.2 slice_reduce_fusion
  4.5 0.2 reduce-window.19
  4.6 0.1 maximum_bitcast_fusion
  4.7 0.2 slice_reduce_fusion.2
  5.0 0.1 pad_maximum_fusion.1
  5.0 0.7 broadcast_in_dim.12.meta_ref
  5.7 0.0 copy-done
  5.7 0.1 subtract_exponential_fusion
  5.8 1.3 broadcast_in_dim.14.fgain_ref
  7.1 1.0 copy.26
  8.1 226.9 %block.1 = bf16[1024,512]{1,0:T(8,128)(2,1)} custom-call(bf16[1024,256]{1,0:T(8,128)(2,1)} %q_ref.1, bf16[1024,256]{1,0:T(8,128)(2,1)} %k_ref.1, bf16[1024,512]{1,0:T(8,128)(2,1)} %v_ref.1, bf16[1024,512]{1,0:T(8,128)(2,1)} %open_ref.1, f32[2,1024]{1,0:T(2,128)} %copy-done, f32[1024,4]{1,0:T(8,128)} %bitcast.24, f32[8,256]{1,0:T(8,128)} %broadcast_in_dim.12.meta_ref, ...), custom_call_target="tpu_custom_call" | custom-call | flops 22000001024 | bytes 10000000 | tf_op jit(solution)/shard_map/block/pallas_call | solution.py:882
  235.0 2.3 copy.42
  (7 shorter events, 0.0 us)
Async XLA Ops:
  3.7 2.0 copy-start

commit v2 on v1

--- a/solution.py
+++ b/solution.py
@@ -218,25 +218,32 @@
 
 def block_body(
     planes,
-    q_ref,
-    k_ref,
-    v_ref,
-    open_ref,
+    q_in,
+    k_in,
+    v_in,
+    open_in,
+    input_in,
+    forget_in,
+    extra_in,
+    resid_in,
+    gain_ref,
+    wo_in,
+    fgain_ref,
+    gate_in,
+    up_in,
+    down_ref,
+    out_ref,
+    gate_ref,
+    up_ref,
+    wo_ref,
     a_ref,
     cols_ref,
     meta_ref,
-    resid_ref,
-    gain_ref,
-    wo_ref,
-    fgain_ref,
-    gate_ref,
-    up_ref,
-    down_ref,
-    out_ref,
     gu,
     dn,
     rows_all,
     hid,
+    sums,
     gu_out,
     num,
     ent,
@@ -251,7 +258,6 @@
     pool,
     core_in,
     x_in,
-    normed,
     core_back,
     y_back,
     x_back,
@@ -266,9 +272,9 @@
 ):
     sp, tp = lax.axis_index("sp"), lax.axis_index("tp")
     z, y, x, c = sp // NY, sp % NY, tp // 2, tp % 2
-    tokens, heads = q_ref.shape[0], a_ref.shape[0]
-    dk, dv = q_ref.shape[1] // heads, v_ref.shape[1] // heads
-    width = resid_ref.shape[1]
+    tokens, heads = q_in.shape[0], input_in.shape[0]
+    dk, dv = q_in.shape[1] // heads, v_in.shape[1] // heads
+    width = resid_in.shape[1]
     depth, hidden = gate_ref.shape
     half = hidden // NY
     count = 2 * NX
@@ -288,6 +294,23 @@
         return pltpu.make_async_remote_copy(
             src_ref=src, dst_ref=dst, send_sem=sems[0], recv_sem=sems[1], device_id=to, device_id_type=BY_NAME
         )
+
+    q_ref, k_ref = core_back.at[0, 0], core_back.at[0, 1]
+    v_ref, open_ref, resid_ref = core_back.at[1], core_back.at[2], core_back.at[3]
+    loads = {}
+    wanted = [("gate", gate_in, gate_ref), ("up", up_in, up_ref), ("k", k_in, k_ref)]
+    for name, source, kept in (("v", v_in, v_ref), ("q", q_in, q_ref), ("open", open_in, open_ref)):
+        if name == "q":
+            wanted.append((name, source, kept))
+        else:
+            for part in range(2):
+                wanted.append((name + str(part), source.at[:, part * wide : (part + 1) * wide], kept.at[part]))
+    wanted.append(("wo", wo_in, wo_ref))
+    for part in range(2):
+        wanted.append(("resid" + str(part), resid_in.at[:, part * wide : (part + 1) * wide], resid_ref.at[part]))
+    for index, (name, source, kept) in enumerate(wanted):
+        loads[name] = pltpu.make_async_copy(source, kept, lsem.at[index + 1])
+        loads[name].start()
 
     barrier = pltpu.get_barrier_semaphore()
     for to in (partner, x_next, y_next):
@@ -297,6 +320,9 @@
             barrier, inc=1, device_id=on_plane((z + step) % planes), device_id_type=BY_NAME
         )
     pl.semaphore_wait(barrier, planes + 2)
+
+    loads["gate"].wait()
+    loads["up"].wait()
 
     for mine in range(NY):
 
@@ -354,6 +380,16 @@
                 z_arrival(way, dist, chunk).wait_recv()
                 z_copy(way, dist, chunk).start()
 
+    def z_down(rank, dist):
+        for way in range(2):
+
+            @pl.when(z == (rank if way == 0 else last - rank))
+            def _():
+                for chunk in (4, 5):
+                    if dist:
+                        z_arrival(way, dist, chunk).wait_recv()
+                    z_copy(way, dist, chunk).start()
+
     def y_rows(owner, chunk):
         start = (z * NY + owner) * depth + chunk * part_rows
         return pl.ds(pl.multiple_of(start, part_rows), part_rows)
@@ -370,9 +406,37 @@
     own_down = pltpu.make_async_copy(
         down_ref.at[pl.ds(pl.multiple_of(y * half, half), half), :], dn.at[sp], lsem.at[0]
     )
-    own_down.start()
-    y_weight(0).start()
     z_send(0)
+
+    def padded(rows):
+        return jnp.concatenate([rows, jnp.zeros((8 - heads, tokens), jnp.float32)], axis=0)
+
+    lane = lax.broadcasted_iota(jnp.int32, (8, tokens), 1)
+    logits = forget_in[...].astype(jnp.float32)
+    running = padded(
+        jnp.minimum(logits, 0.0) - jnp.log1p(jnp.exp(-jnp.abs(logits))) + extra_in[...]
+    )
+    step = 1
+    while step < tokens:
+        running = running + jnp.where(lane >= step, pltpu.roll(running, step, 1), 0.0)
+        step *= 2
+    a_log = padded(input_in[...].astype(jnp.float32)) - running
+    m_log = a_log
+    step = 1
+    while step < tokens:
+        m_log = jnp.maximum(m_log, jnp.where(lane >= step, pltpu.roll(m_log, step, 1), LOWEST_LOG))
+        step *= 2
+    a_ref[...] = a_log
+    a_top, total = m_log[:, tokens - 1 :], running[:, tokens - 1 :]
+    decay = jnp.exp(a_log - a_top)
+    cols_ref[...] = jnp.concatenate(
+        [decay[0:heads], m_log[0:heads], jnp.zeros((8 - 2 * heads, tokens), jnp.float32)], axis=0
+    ).T
+    meta_ref[...] = jnp.zeros_like(meta_ref)
+    meta_ref[0:heads, :] = jnp.broadcast_to((a_top + total)[0:heads], (heads, meta_ref.shape[1]))
+    meta_ref[heads : 2 * heads, :] = jnp.broadcast_to(total[0:heads], (heads, meta_ref.shape[1]))
+    for name in ("k", "v0", "v1"):
+        loads[name].wait()
 
     for h in range(heads):
         weighed = (
@@ -380,7 +444,7 @@
         ).astype(jnp.bfloat16)
         st_own[h] = lax.dot_general(
             weighed,
-            v_ref[:, h * dv : (h + 1) * dv],
+            v_ref[h],
             (((0,), (0,)), ((), ())),
             preferred_element_type=jnp.float32,
         ).astype(jnp.bfloat16)
@@ -391,9 +455,10 @@
     ]
     for copy in state_y:
         copy.start()
-    y_weight(1).start()
-    y_weight(2).start()
-    z_send(1)
+    for chunk in range(3):
+        y_weight(chunk).start()
+    own_down.start()
+    loads["q"].wait()
 
     def attend(h, i):
         span = (i + 1) * strip
@@ -410,7 +475,7 @@
         weight = jnp.where(col <= row, jnp.exp(jnp.minimum(log_weight, 0.0)), 0.0)
         num[at, h * dv : (h + 1) * dv] = jnp.dot(
             (scores * weight).astype(jnp.bfloat16),
-            v_ref[0:span, h * dv : (h + 1) * dv],
+            v_ref[h, 0:span, :],
             preferred_element_type=jnp.float32,
         )
 
@@ -453,13 +518,12 @@
             for copy in state_z(step, z):
                 copy.start()
 
-    for chunk in range(2):
-        y_weight(chunk).wait_recv()
-        z_send(2 + chunk)
-
+    z_send(1)
     for h in range(heads):
         for i in range(1, 4):
             attend(h, i)
+    y_weight(0).wait_recv()
+    z_send(2)
 
     low = jnp.full((heads, meta_ref.shape[1]), LOWEST_LOG, jnp.float32)
     later = jnp.where(y == 1, meta_y[heads : 2 * heads, :], 0.0)
@@ -488,9 +552,8 @@
                 part = st_z[source, h] if source < planes - 1 else st_y[h]
                 ent[h] += part.astype(jnp.float32) * scale[h : h + 1]
 
-    z_forward(1, 0)
-    z_forward(1, 1)
-    z_forward(1, 2)
+    for name in ("open0", "open1", "wo"):
+        loads[name].wait()
 
     def front_core(i):
         at = pl.ds(pl.multiple_of(i * strip, strip), strip)
@@ -521,8 +584,8 @@
                 + jnp.exp(ctop[h : h + 1, 0:1] - m_all) * before
             ) * dk ** (-0.5)
             normal = memory * lax.rsqrt(jnp.mean(memory * memory, axis=-1, keepdims=True) + EPSILON)
-            opened = jax.nn.sigmoid(open_ref[at, lanes].astype(jnp.float32))
-            gated.append((normal * gain_ref[0:1, lanes].astype(jnp.float32) * opened).astype(jnp.bfloat16))
+            opened = jax.nn.sigmoid(open_ref[h, at, :].astype(jnp.float32))
+            gated.append((normal * gain_ref[lanes][None, :].astype(jnp.float32) * opened).astype(jnp.bfloat16))
         gated = jnp.concatenate(gated, axis=1)
         for chip in range(NX):
             for part in range(2):
@@ -552,18 +615,27 @@
         def _():
             gate_strip(i)
 
+        @pl.when(i == 2)
+        def _():
+            y_weight(1).wait_recv()
+            z_send(3)
+
         @pl.when(i >= 1)
         def _():
             core_sum(i - 1)
 
-    z_forward(1, 3)
-    z_forward(2, 0)
+    z_forward(1, 0)
+    z_forward(1, 1)
     y_weight(2).wait_recv()
     own_down.wait()
+    z_down(0, 0)
+    for part in range(2):
+        loads["resid" + str(part)].wait()
 
     def piece(owner_x, owner_c, owner_y, i):
         at = pl.multiple_of(owner_y * tokens + i * strip, strip)
-        return rows_all.at[owner_x * 2 + owner_c, pl.ds(at, strip), :]
+        lanes = pl.multiple_of((owner_x * 2 + owner_c) * width, width)
+        return rows_all.at[pl.ds(at, strip), pl.ds(lanes, width)]
 
     def to_x(i):
         part = piece(x, c, y, i)
@@ -592,14 +664,20 @@
                 + core_in[near, at, :].astype(jnp.float32)
                 + x_in[part, at, :].astype(jnp.float32)
             )
-            rows_all[tp, pl.ds(start, strip), lanes] = (
-                resid_ref[at, lanes].astype(jnp.float32) + total
-            ).astype(jnp.bfloat16)
+            fresh = (resid_ref[part, at, :].astype(jnp.float32) + total).astype(jnp.bfloat16)
+            out_ref[at, lanes] = fresh
+            columns = pl.ds(pl.multiple_of(tp * width + part * wide, wide), wide)
+            rows_all[pl.ds(start, strip), columns] = fresh
         to_x(i).start()
         to_y(0, i).start()
         to_core(0, i).start()
 
-    z_forward(2, 1)
+        @pl.when(i == 1)
+        def _():
+            z_forward(1, 2)
+
+    z_forward(1, 3)
+    z_down(1, 0)
 
     @pl.loop(0, 4)
     def _(i):
@@ -607,10 +685,13 @@
         to_y(1, i).start()
         to_core(1, i).start()
 
+        @pl.when(i == 1)
+        def _():
+            z_forward(2, 0)
+            z_forward(2, 1)
+
     z_forward(2, 2)
-    z_forward(2, 3)
-    z_send(4)
-    z_send(5)
+    z_down(1, 1)
 
     @pl.loop(0, 4)
     def _(i):
@@ -622,17 +703,8 @@
         to_y(1, i).wait_recv()
         to_core(3, i).start()
 
-    for dist in range(1, planes - 1):
-        for chunk in (4, 5):
-            z_forward(dist, chunk)
-
-    for way in range(2):
-        for dist in range(1, planes):
-
-            @pl.when(jnp.logical_and(has_origin(way, dist), jnp.logical_not(has_next(way))))
-            def _():
-                for chunk in range(4):
-                    z_arrival(way, dist, chunk).wait_recv()
+    z_forward(2, 3)
+    z_down(2, 0)
 
     @pl.loop(0, 4)
     def _(i):
@@ -646,53 +718,90 @@
         for kind in range(4):
             to_core(kind, i).wait_send()
 
-    tall = normed.shape[0]
+    short = 32
+
+    @pl.loop(0, NY * tokens // short)
+    def _(i):
+        at = pl.ds(pl.multiple_of(i * short, short), short)
+        wide_rows = rows_all[at, :].astype(jnp.float32)
+        scale = lax.rsqrt(jnp.mean(wide_rows * wide_rows, axis=-1, keepdims=True) + EPSILON)
+        rows_all[at, :] = (wide_rows * scale * fgain_ref[...][None, :].astype(jnp.float32)).astype(
+            jnp.bfloat16
+        )
+
+    tall = 512
+    plane_rows = NY * depth
+    early = last * plane_rows
+    early_at = jnp.where(z == last, plane_rows, 0)
+    late_at = jnp.where(z == last, 0, early)
+
+    def gate_up(i, start, size):
+        at = pl.ds(pl.multiple_of(i * tall, tall), tall)
+        taken = pl.ds(pl.multiple_of(start, plane_rows), size)
+        return at, jnp.dot(rows_all[at, taken], gu[taken, :], preferred_element_type=jnp.float32)
+
+    def gu_arrived(dist):
+        for way in range(2):
+
+            @pl.when(jnp.logical_and(has_origin(way, dist), jnp.logical_not(has_next(way))))
+            def _():
+                for chunk in range(4):
+                    z_arrival(way, dist, chunk).wait_recv()
+
+    for dist in range(1, last):
+        gu_arrived(dist)
 
     @pl.loop(0, NY * tokens // tall)
     def _(i):
-        base = pl.multiple_of(i * tall, tall)
-
-        @pl.loop(0, tall // 64)
-        def _(r):
-            at = pl.ds(pl.multiple_of(base + r * 64, 64), 64)
-            parts = [rows_all[j, at, :].astype(jnp.float32) for j in range(count)]
-            square = sum(jnp.sum(p * p, axis=-1, keepdims=True) for p in parts)
-            scale = lax.rsqrt(square / (count * width) + EPSILON)
-            to = pl.ds(pl.multiple_of(r * 64, 64), 64)
-            for j in range(count):
-                lanes = slice(j * width, (j + 1) * width)
-                normed[to, lanes] = (parts[j] * scale * fgain_ref[0:1, lanes].astype(jnp.float32)).astype(
-                    jnp.bfloat16
-                )
-
-        both = jnp.dot(normed[...], gu[...], preferred_element_type=jnp.float32)
-        hid[pl.ds(base, tall), :] = (jax.nn.silu(both[:, :half]) * both[:, half:]).astype(jnp.bfloat16)
-
-    units = planes * NY
+        at, product = gate_up(i, early_at, early)
+        sums[at, :] = product
+
+    gu_arrived(last)
+
+    @pl.loop(0, NY * tokens // tall)
+    def _(i):
+        at, product = gate_up(i, late_at, plane_rows)
+        both = sums[at, :] + product
+        hid[at, :] = (jax.nn.silu(both[:, :half]) * both[:, half:]).astype(jnp.bfloat16)
+
+    z_down(2, 1)
+    z_down(2, 2)
+
+    units = planes * NY * 2
+    rows = tokens // 2
+
+    def side_of(unit):
+        return unit // 2 % NY
 
     def place(unit):
-        step = unit // NY
-        low_bit = (z % 2 + step % 2) % 2
-        high = (z // 2 + step // 2) % 2
-        return high * 2 + low_bit
+        step = unit // (2 * NY)
+        inner = jnp.where(step < planes - 1, (step + 1) % (planes - 1), step)
+        base = jnp.where(jnp.logical_or(z == 0, z == last), step, inner)
+        return jnp.where(z < planes // 2, base, last - base)
 
     def slot(unit):
-        return unit // 4 * 2 + unit % 2
+        return unit // 8 * 2 + side_of(unit)
+
+    def strip_of(unit):
+        return pl.ds(pl.multiple_of(unit % 2 * rows, rows), rows)
+
+    def held(unit, top_row):
+        return unit // 2 * 2 + top_row, strip_of(unit)
+
+    def both_of(unit):
+        return pool.at[pl.ds(unit // 2 * 2, 2), strip_of(unit)]
 
     def back_core(unit):
-        return remote(
-            pool.at[pl.ds(unit * 2, 2)], core_back.at[slot(unit)], (bsem.at[0, unit], bsem.at[1, unit]), partner
-        )
+        kept = core_back.at[slot(unit), :, strip_of(unit)]
+        return remote(both_of(unit), kept, (bsem.at[0, unit], bsem.at[1, unit]), partner)
 
     def back_y(unit):
-        return remote(
-            pool.at[unit * 2 + 1 - y], y_back.at[slot(unit)], (bsem.at[2, unit], bsem.at[3, unit]), y_next
-        )
+        kept = y_back.at[slot(unit), strip_of(unit)]
+        return remote(pool.at[held(unit, 1 - y)], kept, (bsem.at[2, unit], bsem.at[3, unit]), y_next)
 
     def back_x(unit):
-        return remote(
-            pool.at[unit * 2 + y], x_back.at[unit % 2], (bsem.at[4, unit], bsem.at[5, unit]), x_next
-        )
+        kept = x_back.at[side_of(unit), strip_of(unit)]
+        return remote(pool.at[held(unit, y)], kept, (bsem.at[4, unit], bsem.at[5, unit]), x_next)
 
     def keeps(unit):
         return place(unit) % 2 == c
@@ -703,24 +812,26 @@
     def passes(unit):
         return jnp.logical_and(keeps(unit), place(unit) // 2 != x)
 
+    def add(unit, top_row, other):
+        at = held(unit, top_row)
+        pool[at] = (pool[at].astype(jnp.float32) + other.astype(jnp.float32)).astype(jnp.bfloat16)
+
     def down_part(unit):
-        step, side = unit // NY, unit % NY
-
-        @pl.when(jnp.logical_and(step > 0, jnp.logical_or(z == 0, z == last)))
-        def _():
-            at = place(unit) * NY + side
+        step, side = unit // (2 * NY), side_of(unit)
+        ends = jnp.logical_or(z == 0, z == last)
+
+        @pl.when(jnp.logical_and(jnp.logical_and(step > 0, unit % 2 == 0), ends))
+        def _():
             way = jnp.where(z == 0, 1, 0)
-            part = dn.at[at]
-            remote(part, part, (zs.at[way, step, 4 + side], zr.at[way, step, 4 + side]), on_plane(z)).wait_recv()
+            part = dn.at[place(unit) * NY + side]
+            remote(part, part, (zs.at[way, 0, 4 + side], zr.at[way, step, 4 + side]), on_plane(z)).wait_recv()
 
         weight = dn[place(unit) * NY + side]
-        for top_row in range(NY):
-            for quarter in range(2):
-                rows = tokens // 2
-                start = top_row * tokens + quarter * rows
-                pool[unit * 2 + top_row, pl.ds(quarter * rows, rows), :] = jnp.dot(
-                    hid[pl.ds(start, rows), :], weight, preferred_element_type=jnp.float32
-                ).astype(jnp.bfloat16)
+        for top_row in (1 - y, y):
+            start = pl.multiple_of(top_row * tokens + unit % 2 * rows, rows)
+            pool[held(unit, top_row)] = jnp.dot(
+                hid[pl.ds(start, rows), :], weight, preferred_element_type=jnp.float32
+            ).astype(jnp.bfloat16)
 
         @pl.when(jnp.logical_not(keeps(unit)))
         def _():
@@ -730,20 +841,15 @@
         @pl.when(keeps(unit))
         def _():
             back_core(unit).wait_recv()
-            for side in (1 - y, y):
-                pool[unit * 2 + side] = (
-                    pool[unit * 2 + side].astype(jnp.float32)
-                    + core_back[slot(unit), side].astype(jnp.float32)
-                ).astype(jnp.bfloat16)
+            for top_row in (1 - y, y):
+                add(unit, top_row, core_back[slot(unit), top_row, strip_of(unit)])
             back_y(unit).start()
 
     def after_y(unit):
         @pl.when(keeps(unit))
         def _():
             back_y(unit).wait_recv()
-            pool[unit * 2 + y] = (
-                pool[unit * 2 + y].astype(jnp.float32) + y_back[slot(unit)].astype(jnp.float32)
-            ).astype(jnp.bfloat16)
+            add(unit, y, y_back[slot(unit), strip_of(unit)])
 
         @pl.when(passes(unit))
         def _():
@@ -753,30 +859,36 @@
         @pl.when(owns(unit))
         def _():
             back_x(unit).wait_recv()
-            total = pool[unit * 2 + y].astype(jnp.float32) + x_back[unit % 2].astype(jnp.float32)
-            lanes = pl.ds(pl.multiple_of((unit % 2) * wide, wide), wide)
-            mine = pl.ds(pl.multiple_of(y * tokens, tokens), tokens)
-            out_ref[:, lanes] = (
-                rows_all[tp, mine, lanes].astype(jnp.float32) + 0.5 * total
-            ).astype(out_ref.dtype)
-
-    @pl.loop(0, units + 3)
-    def _(i):
-        @pl.when(i < units)
-        def _():
-            down_part(i)
-
-        @pl.when(jnp.logical_and(i >= 1, i < units + 1))
-        def _():
-            after_core(i - 1)
-
-        @pl.when(jnp.logical_and(i >= 2, i < units + 2))
-        def _():
-            after_y(i - 2)
-
-        @pl.when(i >= 3)
-        def _():
-            after_x(i - 3)
+            at = strip_of(unit)
+            lanes = pl.ds(pl.multiple_of(side_of(unit) * wide, wide), wide)
+            total = pool[held(unit, y)].astype(jnp.float32) + x_back[side_of(unit), at].astype(jnp.float32)
+            out_ref[at, lanes] = (out_ref[at, lanes].astype(jnp.float32) + 0.5 * total).astype(out_ref.dtype)
+
+    def run(low, high):
+        @pl.loop(low, high + 1)
+        def _(i):
+            @pl.when(i < high)
+            def _():
+                down_part(i)
+
+            @pl.when(i > low)
+            def _():
+                after_core(i - 1)
+
+    def each(stage, low, high):
+        @pl.loop(low, high)
+        def _(i):
+            stage(i)
+
+    run(0, 8)
+    each(after_y, 0, 4)
+    run(8, 12)
+    each(after_y, 4, 8)
+    run(12, 14)
+    each(after_y, 8, 12)
+    run(14, units)
+    each(after_y, 12, units)
+    each(after_x, 0, units)
 
     @pl.loop(0, units)
     def _(i):
@@ -835,22 +947,20 @@
     depth, hidden = gate_projection_weight.shape
     half = hidden // NY
     dk, dv = queries.shape[1] // heads, cell_value_rows.shape[1] // heads
-    log_forget = jax.nn.log_sigmoid(forget_gate_logits.astype(jnp.float32)) + forget_extra_term
-    running = jnp.cumsum(log_forget, axis=-1)
-    a_log = input_gate_logits.astype(jnp.float32) - running
-    m_log = lax.cummax(a_log, axis=1)
-    a_top, total = m_log[:, -1], running[:, -1]
-    decay = jnp.exp(a_log - a_top[:, None])
-    cols = jnp.concatenate([decay, m_log], axis=0).T
-    meta = jnp.concatenate([a_top + total, total, jnp.zeros((8 - 2 * heads,), jnp.float32)])
-    meta = jnp.broadcast_to(meta[:, None], (8, dv))
     bf16, f32 = jnp.bfloat16, jnp.float32
     vmem, dma = pltpu.VMEM, pltpu.SemaphoreType.DMA
     scratch = [
+        vmem((depth, hidden), bf16),
+        vmem((depth, hidden), bf16),
+        vmem((heads * dv, model), bf16),
+        vmem((8, tokens), f32),
+        vmem((tokens, 8), f32),
+        vmem((8, dv), f32),
         vmem((model, hidden), bf16),
         vmem((planes * NY, half, depth), bf16),
-        vmem((2 * NX, NY * tokens, width), bf16),
+        vmem((NY * tokens, 2 * NX * width), bf16),
         vmem((NY * tokens, half), bf16),
+        vmem((NY * tokens, hidden), f32),
         vmem((depth, hidden), bf16),
         vmem((tokens, heads * dv), f32),
         vmem((heads, dk, dv), f32),
@@ -865,7 +975,6 @@
         vmem((2 * planes * NY, tokens, width // 2), bf16),
         vmem((4, tokens, width // 2), bf16),
         vmem((2, tokens, width // 2), bf16),
-        vmem((512, model), bf16),
         vmem((planes * NY // 2, 2, tokens, width // 2), bf16),
         vmem((planes * NY // 2, tokens, width // 2), bf16),
         vmem((2, tokens, width // 2), bf16),
@@ -875,14 +984,15 @@
         dma((6, planes)),
         dma((4, 4)),
         dma((14, 4)),
-        dma((6, planes * NY)),
-        dma((1,)),
+        dma((6, planes * NY * 2)),
+        dma((12,)),
     ]
     whole = pl.BlockSpec(memory_space=pltpu.VMEM)
+    far = pl.BlockSpec(memory_space=pl.ANY)
     return pl.pallas_call(
         functools.partial(block_body, planes),
         out_shape=jax.ShapeDtypeStruct((tokens, width), bf16),
-        in_specs=[whole] * 14,
+        in_specs=[far] * 4 + [whole] * 3 + [far, whole, far, whole] + [far] * 3,
         out_specs=whole,
         scratch_shapes=scratch,
         compiler_params=pltpu.CompilerParams(
@@ -895,13 +1005,13 @@
         cell_key_rows,
         cell_value_rows,
         output_gate_logits,
-        a_log,
-        cols,
-        meta,
+        input_gate_logits,
+        forget_gate_logits,
+        forget_extra_term,
         residual,
-        head_norm_gain[None, :],
+        head_norm_gain,
         cell_output_weight,
-        feedforward_norm_gain[None, :],
+        feedforward_norm_gain,
         gate_projection_weight,
         up_projection_weight,
         down_projection_weight,

time: 238 us -> 178 us (0.75)
  the two profiles are of different devices: /device:TPU:10 before, /device:TPU:24 now
where the time goes in v2:
time: 178 us; the launch traced here: 175 us
  Pallas kernels  173 us (97%)
  local copies, waits for them, and re-layouts  2.26 us (1%)
    pallas_call x1, Pallas kernels, plane_layer(): pl.pallas_call(functools.partial(block_body, planes), out_shape=jax.Shape...  173 us

profile of v2, /device:TPU:24, one launch (start us, length us, event | category | flops | bytes accessed | tf_op | source)
XLA Modules:
  0.0 175.3 jit_solution(8812217732711885454)
XLA Ops:
  0.0 173.1 %block.1 = bf16[1024,512]{1,0:T(8,128)(2,1)} custom-call(bf16[1024,256]{1,0:T(8,128)(2,1)} %q_in.1, bf16[1024,256]{1,0:T(8,128)(2,1)} %k_in.1, bf16[1024,512]{1,0:T(8,128)(2,1)} %v_in.1, bf16[1024,512]{1,0:T(8,128)(2,1)} %open_in.1, bf16[2,1024]{1,0:T(2,128)(2,1)} %input_in.1, bf16[2,1024]{1,0:T(2,128)(2,1)} %forget_in.1, f32[2,1024]{1,0:T(2,128)} %extra_in.1, ...), custom_call_target="tpu_custom_call" | custom-call | flops 22000001024 | bytes 10000000 | tf_op jit(solution)/shard_map/block/pallas_call | solution.py:992
  173.1 2.3 %copy.16 = bf16[1024,512]{1,0:T(8,128)(2,1)} copy(bf16[1024,512]{1,0:T(8,128)(2,1)} %block.1) | data formatting | bytes 2097152

commit v3 on v2

--- a/solution.py
+++ b/solution.py
@@ -250,9 +250,11 @@
     st_own,
     st_y,
     st_sum,
+    st_pre,
     st_z,
     meta_y,
     meta_sum,
+    meta_pre,
     meta_z,
     lw_ref,
     pool,
@@ -315,11 +317,14 @@
     barrier = pltpu.get_barrier_semaphore()
     for to in (partner, x_next, y_next):
         pl.semaphore_signal(barrier, inc=1, device_id=to, device_id_type=BY_NAME)
-    for step in range(1, planes):
-        pl.semaphore_signal(
-            barrier, inc=1, device_id=on_plane((z + step) % planes), device_id_type=BY_NAME
-        )
-    pl.semaphore_wait(barrier, planes + 2)
+    for ok, at in ((z > 0, z - 1), (z < last, z + 1)):
+
+        @pl.when(ok)
+        def _():
+            pl.semaphore_signal(barrier, inc=1, device_id=on_plane(at), device_id_type=BY_NAME)
+
+    ends = jnp.logical_or(z == 0, z == last)
+    pl.semaphore_wait(barrier, 5 - jnp.where(ends, 1, 0))
 
     loads["gate"].wait()
     loads["up"].wait()
@@ -343,7 +348,7 @@
     def z_copy(way, dist, chunk):
         at = z - dist if way == 0 else z + dist
         to = z + 1 if way == 0 else z - 1
-        sems = (zs.at[way, dist, chunk], zr.at[way, dist + 1, chunk])
+        sems = (zs.at[way, dist, chunk], zr.at[way, dist, chunk])
         if chunk < 4:
             part = gu.at[gu_rows(at, chunk), :]
         else:
@@ -352,7 +357,7 @@
 
     def z_arrival(way, dist, chunk):
         at = z - dist if way == 0 else z + dist
-        sems = (zs.at[way, dist, chunk], zr.at[way, dist, chunk])
+        sems = (zs.at[way, 0, chunk], zr.at[way, dist - 1, chunk])
         if chunk < 4:
             part = gu.at[gu_rows(at, chunk), :]
         else:
@@ -365,10 +370,10 @@
     def has_origin(way, dist):
         return z >= dist if way == 0 else z + dist <= last
 
-    def z_send(chunk):
-        for way in range(2):
-
-            @pl.when(has_next(way))
+    def z_send(chunk, ways=((0, True), (1, True))):
+        for way, also in ways:
+
+            @pl.when(jnp.logical_and(has_next(way), also))
             def _():
                 z_copy(way, 0, chunk).start()
 
@@ -450,8 +455,8 @@
         ).astype(jnp.bfloat16)
 
     state_y = [
-        remote(st_own, st_y, (ssem.at[0, 0], ssem.at[0, 1]), y_next),
-        remote(meta_ref, meta_y, (ssem.at[1, 0], ssem.at[1, 1]), y_next),
+        remote(st_own, st_y, (ssem.at[0], ssem.at[1]), y_next),
+        remote(meta_ref, meta_y, (ssem.at[2], ssem.at[3]), y_next),
     ]
     for copy in state_y:
         copy.start()
@@ -503,53 +508,78 @@
             + st_y[h].astype(jnp.float32) * scale_other[h : h + 1]
         ).astype(jnp.bfloat16)
 
-    def state_z(step, source):
-        kept = st_z.at[source], meta_z.at[source]
+    def state_z(step, summed):
+        state, meta = (st_pre, meta_pre) if summed else (st_sum, meta_sum)
         to = on_plane(z + step)
         return [
-            remote(st_sum, kept[0], (ssem.at[2, step], ssem.at[3, source]), to),
-            remote(meta_sum, kept[1], (ssem.at[4, step], ssem.at[5, source]), to),
+            remote(state, st_z, (ssem.at[4], ssem.at[5]), to),
+            remote(meta, meta_z, (ssem.at[6], ssem.at[7]), to),
         ]
 
-    for step in range(1, planes):
-
-        @pl.when(z + step <= last)
-        def _():
-            for copy in state_z(step, z):
-                copy.start()
-
-    z_send(1)
+    @pl.when(z == 0)
+    def _():
+        for copy in state_z(1, 0):
+            copy.start()
+
+    def hop():
+        for copy in state_z(0, 0):
+            copy.wait_recv()
+        before, own = meta_z[0:heads, :] + meta_sum[heads : 2 * heads, :], meta_sum[0:heads, :]
+        joint = jnp.maximum(before, own)
+        meta_pre[...] = jnp.zeros_like(meta_pre)
+        meta_pre[0:heads, :] = joint
+        meta_pre[heads : 2 * heads, :] = meta_z[heads : 2 * heads, :] + meta_sum[heads : 2 * heads, :]
+        scale_before, scale_own = jnp.exp(before - joint), jnp.exp(own - joint)
+        for h in range(heads):
+            st_pre[h] = (
+                st_z[h].astype(jnp.float32) * scale_before[h : h + 1]
+                + st_sum[h].astype(jnp.float32) * scale_own[h : h + 1]
+            ).astype(jnp.bfloat16)
+        for copy in state_z(1, 1):
+            copy.start()
+
+    z_send(1, ((0, z != 1), (1, True)))
     for h in range(heads):
         for i in range(1, 4):
             attend(h, i)
+
+    pl.when(z == 1)(hop)
+    z_send(1, ((0, z == 1),))
+
+    def z_half(part):
+        short_part = part_rows // 2
+        start = pl.multiple_of((z * NY + 1 - y) * depth + part * short_part, short_part)
+        piece = gu.at[pl.ds(start, short_part), :]
+        return remote(piece, piece, (zs.at[0, 0, 2], zr.at[0, 0, 2]), on_plane(z + 1))
+
     y_weight(0).wait_recv()
-    z_send(2)
+    z_send(2, ((0, z < 2), (1, True)))
+
+    @pl.when(z == 2)
+    def _():
+        z_half(0).start()
+        hop()
+        z_half(1).start()
 
     low = jnp.full((heads, meta_ref.shape[1]), LOWEST_LOG, jnp.float32)
     later = jnp.where(y == 1, meta_y[heads : 2 * heads, :], 0.0)
-    lw_ref[planes - 1, 0:heads, :] = jnp.where(y == 1, meta_y[0:heads, :], low)
-    ctop = lw_ref[planes - 1, 0:heads, :]
-    for source in range(planes - 2, -1, -1):
-        valid = z > source
-
-        @pl.when(valid)
-        def _():
-            for copy in state_z(0, source):
-                copy.wait_recv()
-
-        here = jnp.where(valid, meta_z[source, 0:heads, :] + later, low)
-        lw_ref[source, 0:heads, :] = here
-        ctop = jnp.maximum(ctop, here)
-        later = later + jnp.where(valid, meta_z[source, heads : 2 * heads, :], 0.0)
+    lw_ref[1, 0:heads, :] = jnp.where(y == 1, meta_y[0:heads, :], low)
+
+    @pl.when(z == last)
+    def _():
+        for copy in state_z(0, 0):
+            copy.wait_recv()
+
+    lw_ref[0, 0:heads, :] = jnp.where(z > 0, meta_z[0:heads, :] + later, low)
+    ctop = jnp.maximum(lw_ref[0, 0:heads, :], lw_ref[1, 0:heads, :])
     ent[...] = jnp.zeros_like(ent)
-    for source in range(planes):
-        valid = z > source if source < planes - 1 else y == 1
+    for source, valid in ((0, z > 0), (1, y == 1)):
 
         @pl.when(valid)
         def _():
             scale = jnp.exp(lw_ref[source, 0:heads, :] - ctop)
             for h in range(heads):
-                part = st_z[source, h] if source < planes - 1 else st_y[h]
+                part = st_y[h] if source else st_z[h]
                 ent[h] += part.astype(jnp.float32) * scale[h : h + 1]
 
     for name in ("open0", "open1", "wo"):
@@ -684,6 +714,8 @@
         to_x(i).wait_recv()
         to_y(1, i).start()
         to_core(1, i).start()
+        to_y(0, i).wait_recv()
+        to_core(2, i).start()
 
         @pl.when(i == 1)
         def _():
@@ -693,10 +725,22 @@
     z_forward(2, 2)
     z_down(1, 1)
 
-    @pl.loop(0, 4)
-    def _(i):
-        to_y(0, i).wait_recv()
-        to_core(2, i).start()
+    short = 128
+
+    def norm_rows(owner, kinds):
+        @pl.loop(0, 4)
+        def _(i):
+            for kind in kinds:
+                to_core(kind, i).wait_recv()
+
+        @pl.loop(0, tokens // short)
+        def _(i):
+            at = pl.ds(pl.multiple_of(owner * tokens + i * short, short), short)
+            wide_rows = rows_all[at, :].astype(jnp.float32)
+            scale = lax.rsqrt(jnp.mean(wide_rows * wide_rows, axis=-1, keepdims=True) + EPSILON)
+            rows_all[at, :] = (wide_rows * scale * fgain_ref[...][None, :].astype(jnp.float32)).astype(
+                jnp.bfloat16
+            )
 
     @pl.loop(0, 4)
     def _(i):
@@ -705,11 +749,6 @@
 
     z_forward(2, 3)
     z_down(2, 0)
-
-    @pl.loop(0, 4)
-    def _(i):
-        for kind in range(4):
-            to_core(kind, i).wait_recv()
 
     @pl.loop(0, 4)
     def _(i):
@@ -718,16 +757,8 @@
         for kind in range(4):
             to_core(kind, i).wait_send()
 
-    short = 32
-
-    @pl.loop(0, NY * tokens // short)
-    def _(i):
-        at = pl.ds(pl.multiple_of(i * short, short), short)
-        wide_rows = rows_all[at, :].astype(jnp.float32)
-        scale = lax.rsqrt(jnp.mean(wide_rows * wide_rows, axis=-1, keepdims=True) + EPSILON)
-        rows_all[at, :] = (wide_rows * scale * fgain_ref[...][None, :].astype(jnp.float32)).astype(
-            jnp.bfloat16
-        )
+    norm_rows(y, (0, 1))
+    norm_rows(1 - y, (2, 3))
 
     tall = 512
     plane_rows = NY * depth
@@ -775,13 +806,22 @@
 
     def place(unit):
         step = unit // (2 * NY)
-        inner = jnp.where(step < planes - 1, (step + 1) % (planes - 1), step)
-        base = jnp.where(jnp.logical_or(z == 0, z == last), step, inner)
+        base = jnp.where(jnp.logical_or(z == 0, z == last), step, (step + 1) % planes)
         return jnp.where(z < planes // 2, base, last - base)
+
+    def across(unit):
+        group = unit // 2
+        return jnp.logical_or(group == 1, group == 4)
+
+    def along(unit):
+        return jnp.logical_not(across(unit))
 
     def slot(unit):
         return unit // 8 * 2 + side_of(unit)
 
+    def kept_index(unit):
+        return slot(unit) * 2 + unit % 2
+
     def strip_of(unit):
         return pl.ds(pl.multiple_of(unit % 2 * rows, rows), rows)
 
@@ -793,15 +833,19 @@
 
     def back_core(unit):
         kept = core_back.at[slot(unit), :, strip_of(unit)]
-        return remote(both_of(unit), kept, (bsem.at[0, unit], bsem.at[1, unit]), partner)
+        return remote(both_of(unit), kept, (bsem.at[0, kept_index(unit)], bsem.at[1, kept_index(unit)]), partner)
 
     def back_y(unit):
         kept = y_back.at[slot(unit), strip_of(unit)]
-        return remote(pool.at[held(unit, 1 - y)], kept, (bsem.at[2, unit], bsem.at[3, unit]), y_next)
+        return remote(pool.at[held(unit, 1 - y)], kept, (bsem.at[2, kept_index(unit)], bsem.at[3, kept_index(unit)]), y_next)
 
     def back_x(unit):
-        kept = x_back.at[side_of(unit), strip_of(unit)]
-        return remote(pool.at[held(unit, y)], kept, (bsem.at[4, unit], bsem.at[5, unit]), x_next)
+        kept = x_back.at[side_of(unit), y, strip_of(unit)]
+        return remote(pool.at[held(unit, y)], kept, (bsem.at[4, unit % 4], bsem.at[4, 4 + unit % 4]), x_next)
+
+    def back_xx(unit):
+        kept = x_back.at[side_of(unit), :, strip_of(unit)]
+        return remote(both_of(unit), kept, (bsem.at[4, unit % 4], bsem.at[4, 4 + unit % 4]), x_next)
 
     def keeps(unit):
         return place(unit) % 2 == c
@@ -824,7 +868,7 @@
         def _():
             way = jnp.where(z == 0, 1, 0)
             part = dn.at[place(unit) * NY + side]
-            remote(part, part, (zs.at[way, 0, 4 + side], zr.at[way, step, 4 + side]), on_plane(z)).wait_recv()
+            remote(part, part, (zs.at[way, 0, 4 + side], zr.at[way, step - 1, 4 + side]), on_plane(z)).wait_recv()
 
         weight = dn[place(unit) * NY + side]
         for top_row in (1 - y, y):
@@ -843,6 +887,21 @@
             back_core(unit).wait_recv()
             for top_row in (1 - y, y):
                 add(unit, top_row, core_back[slot(unit), top_row, strip_of(unit)])
+
+        @pl.when(jnp.logical_and(keeps(unit), along(unit)))
+        def _():
+            back_y(unit).start()
+
+        @pl.when(jnp.logical_and(passes(unit), across(unit)))
+        def _():
+            back_xx(unit).start()
+
+    def after_xx(unit):
+        @pl.when(owns(unit))
+        def _():
+            back_xx(unit).wait_recv()
+            for top_row in (1 - y, y):
+                add(unit, top_row, x_back[side_of(unit), top_row, strip_of(unit)])
             back_y(unit).start()
 
     def after_y(unit):
@@ -855,14 +914,22 @@
         def _():
             back_x(unit).start()
 
-    def after_x(unit):
-        @pl.when(owns(unit))
+    def finish(unit, other):
+        at = strip_of(unit)
+        lanes = pl.ds(pl.multiple_of(side_of(unit) * wide, wide), wide)
+        total = pool[held(unit, y)].astype(jnp.float32) + other.astype(jnp.float32)
+        out_ref[at, lanes] = (out_ref[at, lanes].astype(jnp.float32) + 0.5 * total).astype(out_ref.dtype)
+
+    def after_all(unit):
+        @pl.when(jnp.logical_and(owns(unit), along(unit)))
         def _():
             back_x(unit).wait_recv()
-            at = strip_of(unit)
-            lanes = pl.ds(pl.multiple_of(side_of(unit) * wide, wide), wide)
-            total = pool[held(unit, y)].astype(jnp.float32) + x_back[side_of(unit), at].astype(jnp.float32)
-            out_ref[at, lanes] = (out_ref[at, lanes].astype(jnp.float32) + 0.5 * total).astype(out_ref.dtype)
+            finish(unit, x_back[side_of(unit), y, strip_of(unit)])
+
+        @pl.when(jnp.logical_and(owns(unit), across(unit)))
+        def _():
+            back_y(unit).wait_recv()
+            finish(unit, y_back[slot(unit), strip_of(unit)])
 
     def run(low, high):
         @pl.loop(low, high + 1)
@@ -880,15 +947,30 @@
         def _(i):
             stage(i)
 
+
+    def at_ends(low, high):
+        @pl.when(ends)
+        def _():
+            run(low, high)
+
     run(0, 8)
-    each(after_y, 0, 4)
-    run(8, 12)
+
+    @pl.when(jnp.logical_not(ends))
+    def _():
+        run(8, units)
+
+    each(after_y, 0, 2)
+    each(after_xx, 2, 4)
+    at_ends(8, 10)
     each(after_y, 4, 8)
-    run(12, 14)
-    each(after_y, 8, 12)
-    run(14, units)
+    at_ends(10, 12)
+    each(after_xx, 8, 9)
+    at_ends(12, 14)
+    each(after_y, 10, 12)
+    at_ends(14, units)
+    each(after_xx, 9, 10)
     each(after_y, 12, units)
-    each(after_x, 0, units)
+    each(after_all, 0, units)
 
     @pl.loop(0, units)
     def _(i):
@@ -896,24 +978,31 @@
         def _():
             back_core(i).wait_send()
 
-        @pl.when(keeps(i))
+        @pl.when(jnp.logical_and(keeps(i), jnp.logical_or(along(i), owns(i))))
         def _():
             back_y(i).wait_send()
 
-        @pl.when(passes(i))
+        @pl.when(jnp.logical_and(passes(i), along(i)))
         def _():
             back_x(i).wait_send()
+
+        @pl.when(jnp.logical_and(passes(i), across(i)))
+        def _():
+            back_xx(i).wait_send()
 
     for chunk in range(3):
         y_weight(chunk).wait_send()
     for copy in state_y:
         copy.wait_send()
-    for step in range(1, planes):
-
-        @pl.when(z + step <= last)
-        def _():
-            for copy in state_z(step, z):
-                copy.wait_send()
+    @pl.when(z == 0)
+    def _():
+        for copy in state_z(1, 0):
+            copy.wait_send()
+
+    @pl.when(jnp.logical_and(z > 0, z < last))
+    def _():
+        for copy in state_z(1, 1):
+            copy.wait_send()
 
     for way in range(2):
         for dist in range(planes - 1):
@@ -967,36 +1056,38 @@
         vmem((heads, dk, dv), bf16),
         vmem((heads, dk, dv), bf16),
         vmem((heads, dk, dv), bf16),
-        vmem((planes - 1, heads, dk, dv), bf16),
+        vmem((heads, dk, dv), bf16),
+        vmem((heads, dk, dv), bf16),
         vmem((8, dv), f32),
         vmem((8, dv), f32),
-        vmem((planes - 1, 8, dv), f32),
-        vmem((planes, 8, dv), f32),
+        vmem((8, dv), f32),
+        vmem((8, dv), f32),
+        vmem((2, 8, dv), f32),
         vmem((2 * planes * NY, tokens, width // 2), bf16),
         vmem((4, tokens, width // 2), bf16),
         vmem((2, tokens, width // 2), bf16),
         vmem((planes * NY // 2, 2, tokens, width // 2), bf16),
         vmem((planes * NY // 2, tokens, width // 2), bf16),
-        vmem((2, tokens, width // 2), bf16),
-        dma((2, planes, 6)),
-        dma((2, planes, 6)),
+        vmem((2, 2, tokens, width // 2), bf16),
+        dma((2, planes - 1, 6)),
+        dma((2, planes - 1, 6)),
         dma((2, 3)),
-        dma((6, planes)),
+        dma((8,)),
         dma((4, 4)),
         dma((14, 4)),
-        dma((6, planes * NY * 2)),
+        dma((5, planes * NY)),
         dma((12,)),
     ]
     whole = pl.BlockSpec(memory_space=pltpu.VMEM)
     far = pl.BlockSpec(memory_space=pl.ANY)
     return pl.pallas_call(
         functools.partial(block_body, planes),
-        out_shape=jax.ShapeDtypeStruct((tokens, width), bf16),
+        out_shape=pltpu.VMEM((tokens, width), bf16),
         in_specs=[far] * 4 + [whole] * 3 + [far, whole, far, whole] + [far] * 3,
         out_specs=whole,
         scratch_shapes=scratch,
         compiler_params=pltpu.CompilerParams(
-            collective_id=0, has_side_effects=True, vmem_limit_bytes=67043328
+            collective_id=0, has_side_effects=True, vmem_limit_bytes=65000000
         ),
         cost_estimate=pl.CostEstimate(flops=22 * 10**9, bytes_accessed=10**7, transcendentals=0),
         name="block",

time: 178 us -> 166 us (0.933); the launches traced: 175 us -> 166 us
  Pallas kernels: 173 us -> 165 us
    pallas_call x1, Pallas kernels: 173 us -> 165 us  [plane_layer(): pl.pallas_call(functools.partial(block_body, planes), out_shape=pltpu.VME...]
where the time goes in v3:
time: 166 us
  Pallas kernels  165 us (99%)
    pallas_call x1, Pallas kernels, plane_layer(): pl.pallas_call(functools.partial(block_body, planes), out_shape=pltpu.VME...  165 us

profile of v3, /device:TPU:24, one launch (start us, length us, event | category | flops | bytes accessed | tf_op | source)
XLA Modules:
  0.0 165.9 jit_solution(15393891563693397010)
XLA Ops:
  0.0 164.9 %block.1 = bf16[1024,512]{1,0:T(8,128)(2,1)S(1)} custom-call(bf16[1024,256]{1,0:T(8,128)(2,1)} %q_in.1, bf16[1024,256]{1,0:T(8,128)(2,1)} %k_in.1, bf16[1024,512]{1,0:T(8,128)(2,1)} %v_in.1, bf16[1024,512]{1,0:T(8,128)(2,1)} %open_in.1, bf16[2,1024]{1,0:T(2,128)(2,1)} %input_in.1, bf16[2,1024]{1,0:T(2,128)(2,1)} %forget_in.1, f32[2,1024]{1,0:T(2,128)} %extra_in.1, ...), custom_call_target="tpu_custom_call" | custom-call | flops 22000001024 | bytes 10000000 | tf_op jit(solution)/shard_map/block/pallas_call | solution.py:1083
  164.9 1.0 copy.16

commit v4 on v3

--- a/solution.py
+++ b/solution.py
@@ -213,6 +213,7 @@
 
 
 NX, NY = 2, 2
+PIECES = 4
 BY_NAME = pl.DeviceIdType.MESH
 
 
@@ -348,7 +349,7 @@
     def z_copy(way, dist, chunk):
         at = z - dist if way == 0 else z + dist
         to = z + 1 if way == 0 else z - 1
-        sems = (zs.at[way, dist, chunk], zr.at[way, dist, chunk])
+        sems = (zs.at[way, dist, chunk // 4], zr.at[way, dist, chunk])
         if chunk < 4:
             part = gu.at[gu_rows(at, chunk), :]
         else:
@@ -357,7 +358,7 @@
 
     def z_arrival(way, dist, chunk):
         at = z - dist if way == 0 else z + dist
-        sems = (zs.at[way, 0, chunk], zr.at[way, dist - 1, chunk])
+        sems = (zs.at[way, 0, 0], zr.at[way, dist - 1, chunk])
         if chunk < 4:
             part = gu.at[gu_rows(at, chunk), :]
         else:
@@ -550,7 +551,7 @@
         short_part = part_rows // 2
         start = pl.multiple_of((z * NY + 1 - y) * depth + part * short_part, short_part)
         piece = gu.at[pl.ds(start, short_part), :]
-        return remote(piece, piece, (zs.at[0, 0, 2], zr.at[0, 0, 2]), on_plane(z + 1))
+        return remote(piece, piece, (zs.at[0, 0, 0], zr.at[0, 0, 2]), on_plane(z + 1))
 
     y_weight(0).wait_recv()
     z_send(2, ((0, z < 2), (1, True)))
@@ -588,13 +589,13 @@
     def front_core(i):
         at = pl.ds(pl.multiple_of(i * strip, strip), strip)
         return remote(
-            pool.at[0:4, at, :], core_in.at[:, at, :], (fsem.at[0, i], fsem.at[1, i]), partner
+            pool.at[0:4, at, :], core_in.at[:, at, :], (fsem.at[8], fsem.at[i]), partner
         )
 
     def front_x(i):
         at = pl.ds(pl.multiple_of(i * strip, strip), strip)
         return remote(
-            pool.at[8:10, at, :], x_in.at[:, at, :], (fsem.at[2, i], fsem.at[3, i]), x_next
+            pool.at[8:10, at, :], x_in.at[:, at, :], (fsem.at[9], fsem.at[4 + i]), x_next
         )
 
     def gate_strip(i):
@@ -669,17 +670,17 @@
 
     def to_x(i):
         part = piece(x, c, y, i)
-        return remote(part, part, (gsem.at[0, i], gsem.at[1, i]), x_next)
+        return remote(part, part, (gsem.at[28], gsem.at[i]), x_next)
 
     def to_y(kind, i):
         part = piece(x if kind == 0 else 1 - x, c, y, i)
-        return remote(part, part, (gsem.at[2 + kind, i], gsem.at[4 + kind, i]), y_next)
+        return remote(part, part, (gsem.at[29 + kind], gsem.at[4 + kind * 4 + i]), y_next)
 
     def to_core(kind, i):
         part = piece(
             x if kind % 2 == 0 else 1 - x, c, y if kind // 2 == 0 else 1 - y, i
         )
-        return remote(part, part, (gsem.at[6 + kind, i], gsem.at[10 + kind, i]), partner)
+        return remote(part, part, (gsem.at[31 + kind], gsem.at[12 + kind * 4 + i]), partner)
 
     @pl.loop(0, 4)
     def _(i):
@@ -748,14 +749,12 @@
         to_core(3, i).start()
 
     z_forward(2, 3)
-    z_down(2, 0)
-
-    @pl.loop(0, 4)
-    def _(i):
-        for copy in (front_core(i), front_x(i), to_x(i), to_y(0, i), to_y(1, i)):
-            copy.wait_send()
-        for kind in range(4):
-            to_core(kind, i).wait_send()
+
+    whole_strip = rows_all.at[pl.ds(0, tokens), pl.ds(0, width)]
+    remote(pool.at[0:4], pool.at[0:4], (fsem.at[8], fsem.at[0]), partner).wait_send()
+    remote(pool.at[8:10], pool.at[8:10], (fsem.at[9], fsem.at[4]), x_next).wait_send()
+    for index in range(28, 35):
+        remote(whole_strip, whole_strip, (gsem.at[index], gsem.at[0]), partner).wait_send()
 
     norm_rows(y, (0, 1))
     norm_rows(1 - y, (2, 3))
@@ -787,65 +786,56 @@
         at, product = gate_up(i, early_at, early)
         sums[at, :] = product
 
+    z_down(2, 1)
+    z_down(2, 0)
     gu_arrived(last)
 
-    @pl.loop(0, NY * tokens // tall)
-    def _(i):
+    def finish_hidden(i):
         at, product = gate_up(i, late_at, plane_rows)
         both = sums[at, :] + product
         hid[at, :] = (jax.nn.silu(both[:, :half]) * both[:, half:]).astype(jnp.bfloat16)
 
-    z_down(2, 1)
-    z_down(2, 2)
-
-    units = planes * NY * 2
-    rows = tokens // 2
+    @pl.loop(0, NY)
+    def _(i):
+        finish_hidden(i * (tokens // tall))
+
+
+    units = planes * NY * PIECES
+    rows = tokens // PIECES
 
     def side_of(unit):
-        return unit // 2 % NY
+        return unit // PIECES % NY
 
     def place(unit):
-        step = unit // (2 * NY)
-        base = jnp.where(jnp.logical_or(z == 0, z == last), step, (step + 1) % planes)
-        return jnp.where(z < planes // 2, base, last - base)
-
-    def across(unit):
-        group = unit // 2
-        return jnp.logical_or(group == 1, group == 4)
-
-    def along(unit):
-        return jnp.logical_not(across(unit))
+        step = unit // (PIECES * NY)
+        return (z // 2 + step % 2) % 2 * 2 + (z % 2 + step // 2) % 2
 
     def slot(unit):
-        return unit // 8 * 2 + side_of(unit)
+        return unit // (PIECES * NY) % 2 * 2 + side_of(unit)
 
     def kept_index(unit):
-        return slot(unit) * 2 + unit % 2
+        return slot(unit) * PIECES + unit % PIECES
 
     def strip_of(unit):
-        return pl.ds(pl.multiple_of(unit % 2 * rows, rows), rows)
+        return pl.ds(pl.multiple_of(unit % PIECES * rows, rows), rows)
 
     def held(unit, top_row):
-        return unit // 2 * 2 + top_row, strip_of(unit)
+        return unit // PIECES * 2 + top_row, strip_of(unit)
 
     def both_of(unit):
-        return pool.at[pl.ds(unit // 2 * 2, 2), strip_of(unit)]
+        return pool.at[pl.ds(unit // PIECES * 2, 2), strip_of(unit)]
 
     def back_core(unit):
         kept = core_back.at[slot(unit), :, strip_of(unit)]
-        return remote(both_of(unit), kept, (bsem.at[0, kept_index(unit)], bsem.at[1, kept_index(unit)]), partner)
+        return remote(both_of(unit), kept, (bsem.at[0], bsem.at[3 + kept_index(unit)]), partner)
 
     def back_y(unit):
         kept = y_back.at[slot(unit), strip_of(unit)]
-        return remote(pool.at[held(unit, 1 - y)], kept, (bsem.at[2, kept_index(unit)], bsem.at[3, kept_index(unit)]), y_next)
+        return remote(pool.at[held(unit, 1 - y)], kept, (bsem.at[1], bsem.at[3 + 4 * PIECES + kept_index(unit)]), y_next)
 
     def back_x(unit):
-        kept = x_back.at[side_of(unit), y, strip_of(unit)]
-        return remote(pool.at[held(unit, y)], kept, (bsem.at[4, unit % 4], bsem.at[4, 4 + unit % 4]), x_next)
-
-    def back_xx(unit):
-        kept = x_back.at[side_of(unit), :, strip_of(unit)]
-        return remote(both_of(unit), kept, (bsem.at[4, unit % 4], bsem.at[4, 4 + unit % 4]), x_next)
+        kept = x_back.at[side_of(unit), strip_of(unit)]
+        return remote(pool.at[held(unit, y)], kept, (bsem.at[2], bsem.at[3 + 8 * PIECES + unit % (2 * PIECES)]), x_next)
 
     def keeps(unit):
         return place(unit) % 2 == c
@@ -861,18 +851,20 @@
         pool[at] = (pool[at].astype(jnp.float32) + other.astype(jnp.float32)).astype(jnp.bfloat16)
 
     def down_part(unit):
-        step, side = unit // (2 * NY), side_of(unit)
+        step, side = unit // (PIECES * NY), side_of(unit)
         ends = jnp.logical_or(z == 0, z == last)
 
-        @pl.when(jnp.logical_and(jnp.logical_and(step > 0, unit % 2 == 0), ends))
-        def _():
+        @pl.when(jnp.logical_and(jnp.logical_and(step > 0, unit % PIECES == 0), ends))
+        def _():
+            at = place(unit)
             way = jnp.where(z == 0, 1, 0)
-            part = dn.at[place(unit) * NY + side]
-            remote(part, part, (zs.at[way, 0, 4 + side], zr.at[way, step - 1, 4 + side]), on_plane(z)).wait_recv()
+            dist = jnp.where(z == 0, at, z - at)
+            part = dn.at[at * NY + side]
+            remote(part, part, (zs.at[way, 0, 0], zr.at[way, dist - 1, 4 + side]), on_plane(z)).wait_recv()
 
         weight = dn[place(unit) * NY + side]
         for top_row in (1 - y, y):
-            start = pl.multiple_of(top_row * tokens + unit % 2 * rows, rows)
+            start = pl.multiple_of(top_row * tokens + unit % PIECES * rows, rows)
             pool[held(unit, top_row)] = jnp.dot(
                 hid[pl.ds(start, rows), :], weight, preferred_element_type=jnp.float32
             ).astype(jnp.bfloat16)
@@ -887,21 +879,6 @@
             back_core(unit).wait_recv()
             for top_row in (1 - y, y):
                 add(unit, top_row, core_back[slot(unit), top_row, strip_of(unit)])
-
-        @pl.when(jnp.logical_and(keeps(unit), along(unit)))
-        def _():
-            back_y(unit).start()
-
-        @pl.when(jnp.logical_and(passes(unit), across(unit)))
-        def _():
-            back_xx(unit).start()
-
-    def after_xx(unit):
-        @pl.when(owns(unit))
-        def _():
-            back_xx(unit).wait_recv()
-            for top_row in (1 - y, y):
-                add(unit, top_row, x_back[side_of(unit), top_row, strip_of(unit)])
             back_y(unit).start()
 
     def after_y(unit):
@@ -920,27 +897,28 @@
         total = pool[held(unit, y)].astype(jnp.float32) + other.astype(jnp.float32)
         out_ref[at, lanes] = (out_ref[at, lanes].astype(jnp.float32) + 0.5 * total).astype(out_ref.dtype)
 
-    def after_all(unit):
-        @pl.when(jnp.logical_and(owns(unit), along(unit)))
+    def after_x(unit):
+        @pl.when(owns(unit))
         def _():
             back_x(unit).wait_recv()
-            finish(unit, x_back[side_of(unit), y, strip_of(unit)])
-
-        @pl.when(jnp.logical_and(owns(unit), across(unit)))
-        def _():
-            back_y(unit).wait_recv()
-            finish(unit, y_back[slot(unit), strip_of(unit)])
-
-    def run(low, high):
+            finish(unit, x_back[side_of(unit), strip_of(unit)])
+
+    def run(low, high, begun=0, trail=0):
         @pl.loop(low, high + 1)
         def _(i):
-            @pl.when(i < high)
+            @pl.when(jnp.logical_and(i >= begun, i < high))
             def _():
                 down_part(i)
 
             @pl.when(i > low)
             def _():
                 after_core(i - 1)
+
+            if trail:
+
+                @pl.when(i < high - 1)
+                def _():
+                    after_y(i - trail)
 
     def each(stage, low, high):
         @pl.loop(low, high)
@@ -953,47 +931,53 @@
         def _():
             run(low, high)
 
-    run(0, 8)
+    begun = tall // rows
+
+    @pl.loop(0, begun)
+    def _(i):
+        down_part(i)
+
+    @pl.loop(0, NY)
+    def _(i):
+        finish_hidden(i * (tokens // tall) + 1)
+
+    run(0, 8, begun)
+    z_down(2, 2)
+    run(8, 16)
 
     @pl.when(jnp.logical_not(ends))
     def _():
-        run(8, units)
-
-    each(after_y, 0, 2)
-    each(after_xx, 2, 4)
-    at_ends(8, 10)
-    each(after_y, 4, 8)
-    at_ends(10, 12)
-    each(after_xx, 8, 9)
-    at_ends(12, 14)
-    each(after_y, 10, 12)
-    at_ends(14, units)
-    each(after_xx, 9, 10)
-    each(after_y, 12, units)
-    each(after_all, 0, units)
-
-    @pl.loop(0, units)
-    def _(i):
-        @pl.when(jnp.logical_not(keeps(i)))
-        def _():
-            back_core(i).wait_send()
-
-        @pl.when(jnp.logical_and(keeps(i), jnp.logical_or(along(i), owns(i))))
-        def _():
-            back_y(i).wait_send()
-
-        @pl.when(jnp.logical_and(passes(i), along(i)))
-        def _():
-            back_x(i).wait_send()
-
-        @pl.when(jnp.logical_and(passes(i), across(i)))
-        def _():
-            back_xx(i).wait_send()
-
+        run(16, units)
+
+    each(after_y, 0, 8)
+    at_ends(16, 20)
+    each(after_y, 8, 12)
+    at_ends(20, 24)
+    each(after_y, 12, 20)
+    at_ends(24, 28)
+    each(after_y, 20, 24)
+    each(after_y, units - 2 * PIECES, units - 2 * PIECES + 1)
+
+    @pl.when(ends)
+    def _():
+        run(units - PIECES, units, 0, PIECES - 1)
+
+    @pl.when(jnp.logical_not(ends))
+    def _():
+        each(after_y, units - 2 * PIECES + 1, units - PIECES)
+
+    each(after_y, units - PIECES, units)
+    def sent(part, sem, to):
+        remote(part, part, (sem, zr.at[0, 0, 0]), to).wait_send()
+
+    sent(core_back, bsem.at[0], partner)
+    sent(y_back, bsem.at[1], y_next)
+    sent(x_back, bsem.at[2], x_next)
     for chunk in range(3):
         y_weight(chunk).wait_send()
     for copy in state_y:
         copy.wait_send()
+
     @pl.when(z == 0)
     def _():
         for copy in state_z(1, 0):
@@ -1009,8 +993,10 @@
 
             @pl.when(jnp.logical_and(has_origin(way, dist), has_next(way)))
             def _():
-                for chunk in range(6):
-                    z_copy(way, dist, chunk).wait_send()
+                sent(gu.at[pl.ds(0, plane_rows), :], zs.at[way, dist, 0], partner)
+                sent(dn.at[pl.ds(0, NY)], zs.at[way, dist, 1], partner)
+
+    each(after_x, 0, units)
 
 
 def plane_layer(
@@ -1068,14 +1054,14 @@
         vmem((2, tokens, width // 2), bf16),
         vmem((planes * NY // 2, 2, tokens, width // 2), bf16),
         vmem((planes * NY // 2, tokens, width // 2), bf16),
-        vmem((2, 2, tokens, width // 2), bf16),
-        dma((2, planes - 1, 6)),
+        vmem((2, tokens, width // 2), bf16),
+        dma((2, planes - 1, 2)),
         dma((2, planes - 1, 6)),
         dma((2, 3)),
         dma((8,)),
-        dma((4, 4)),
-        dma((14, 4)),
-        dma((5, planes * NY)),
+        dma((10,)),
+        dma((35,)),
+        dma((3 + 10 * PIECES,)),
         dma((12,)),
     ]
     whole = pl.BlockSpec(memory_space=pltpu.VMEM)

time: 166 us -> 162 us (0.976)
  Pallas kernels: 165 us -> 161 us
    pallas_call x1, Pallas kernels: 165 us -> 161 us  [plane_layer(): pl.pallas_call(functools.partial(block_body, planes), out_shape=pltpu.VME...]
where the time goes in v4:
time: 162 us
  Pallas kernels  161 us (99%)
    pallas_call x1, Pallas kernels, plane_layer(): pl.pallas_call(functools.partial(block_body, planes), out_shape=pltpu.VME...  161 us

profile of v4, /device:TPU:24, one launch (start us, length us, event | category | flops | bytes accessed | tf_op | source)
XLA Modules:
  0.0 162.2 jit_solution(11158635185744817100)
XLA Ops:
  0.0 161.2 %block.1 = bf16[1024,512]{1,0:T(8,128)(2,1)S(1)} custom-call(bf16[1024,256]{1,0:T(8,128)(2,1)} %q_in.1, bf16[1024,256]{1,0:T(8,128)(2,1)} %k_in.1, bf16[1024,512]{1,0:T(8,128)(2,1)} %v_in.1, bf16[1024,512]{1,0:T(8,128)(2,1)} %open_in.1, bf16[2,1024]{1,0:T(2,128)(2,1)} %input_in.1, bf16[2,1024]{1,0:T(2,128)(2,1)} %forget_in.1, f32[2,1024]{1,0:T(2,128)} %extra_in.1, ...), custom_call_target="tpu_custom_call" | custom-call | flops 22000001024 | bytes 10000000 | tf_op jit(solution)/shard_map/block/pallas_call | solution.py:1069
  161.2 1.0 copy.16

commit v5 on v4

--- a/solution.py
+++ b/solution.py
@@ -223,17 +223,22 @@
     k_in,
     v_in,
     open_in,
-    input_in,
-    forget_in,
-    extra_in,
+    input_far,
+    forget_far,
+    extra_far,
     resid_in,
-    gain_ref,
+    gain_far,
     wo_in,
-    fgain_ref,
+    fgain_far,
     gate_in,
     up_in,
     down_ref,
     out_ref,
+    input_in,
+    forget_in,
+    extra_in,
+    gain_ref,
+    fgain_ref,
     gate_ref,
     up_ref,
     wo_ref,
@@ -301,7 +306,16 @@
     q_ref, k_ref = core_back.at[0, 0], core_back.at[0, 1]
     v_ref, open_ref, resid_ref = core_back.at[1], core_back.at[2], core_back.at[3]
     loads = {}
-    wanted = [("gate", gate_in, gate_ref), ("up", up_in, up_ref), ("k", k_in, k_ref)]
+    wanted = [
+        ("gate", gate_in, gate_ref),
+        ("up", up_in, up_ref),
+        ("forget", forget_far, forget_in),
+        ("extra", extra_far, extra_in),
+        ("input", input_far, input_in),
+        ("gain", gain_far, gain_ref),
+        ("fgain", fgain_far, fgain_ref),
+        ("k", k_in, k_ref),
+    ]
     for name, source, kept in (("v", v_in, v_ref), ("q", q_in, q_ref), ("open", open_in, open_ref)):
         if name == "q":
             wanted.append((name, source, kept))
@@ -417,6 +431,8 @@
     def padded(rows):
         return jnp.concatenate([rows, jnp.zeros((8 - heads, tokens), jnp.float32)], axis=0)
 
+    for name in ("forget", "extra", "input", "gain", "fgain"):
+        loads[name].wait()
     lane = lax.broadcasted_iota(jnp.int32, (8, tokens), 1)
     logits = forget_in[...].astype(jnp.float32)
     running = padded(
@@ -670,17 +686,17 @@
 
     def to_x(i):
         part = piece(x, c, y, i)
-        return remote(part, part, (gsem.at[28], gsem.at[i]), x_next)
+        return remote(part, part, (gsem.at[16], gsem.at[i]), x_next)
 
     def to_y(kind, i):
         part = piece(x if kind == 0 else 1 - x, c, y, i)
-        return remote(part, part, (gsem.at[29 + kind], gsem.at[4 + kind * 4 + i]), y_next)
+        return remote(part, part, (gsem.at[17 + kind], gsem.at[4 + kind * 4 + i]), y_next)
 
     def to_core(kind, i):
         part = piece(
             x if kind % 2 == 0 else 1 - x, c, y if kind // 2 == 0 else 1 - y, i
         )
-        return remote(part, part, (gsem.at[31 + kind], gsem.at[12 + kind * 4 + i]), partner)
+        return remote(part, part, (gsem.at[19 + kind], gsem.at[12 + kind]), partner)
 
     @pl.loop(0, 4)
     def _(i):
@@ -729,10 +745,8 @@
     short = 128
 
     def norm_rows(owner, kinds):
-        @pl.loop(0, 4)
-        def _(i):
-            for kind in kinds:
-                to_core(kind, i).wait_recv()
+        for kind in kinds:
+            remote(whole_strip, whole_strip, (gsem.at[16], gsem.at[12 + kind]), partner).wait_recv()
 
         @pl.loop(0, tokens // short)
         def _(i):
@@ -753,7 +767,7 @@
     whole_strip = rows_all.at[pl.ds(0, tokens), pl.ds(0, width)]
     remote(pool.at[0:4], pool.at[0:4], (fsem.at[8], fsem.at[0]), partner).wait_send()
     remote(pool.at[8:10], pool.at[8:10], (fsem.at[9], fsem.at[4]), x_next).wait_send()
-    for index in range(28, 35):
+    for index in range(16, 23):
         remote(whole_strip, whole_strip, (gsem.at[index], gsem.at[0]), partner).wait_send()
 
     norm_rows(y, (0, 1))
@@ -1025,6 +1039,11 @@
     bf16, f32 = jnp.bfloat16, jnp.float32
     vmem, dma = pltpu.VMEM, pltpu.SemaphoreType.DMA
     scratch = [
+        vmem((heads, tokens), input_gate_logits.dtype),
+        vmem((heads, tokens), forget_gate_logits.dtype),
+        vmem((heads, tokens), forget_extra_term.dtype),
+        vmem((heads * dv,), head_norm_gain.dtype),
+        vmem((model,), feedforward_norm_gain.dtype),
         vmem((depth, hidden), bf16),
         vmem((depth, hidden), bf16),
         vmem((heads * dv, model), bf16),
@@ -1060,16 +1079,16 @@
         dma((2, 3)),
         dma((8,)),
         dma((10,)),
-        dma((35,)),
+        dma((23,)),
         dma((3 + 10 * PIECES,)),
-        dma((12,)),
+        dma((17,)),
     ]
     whole = pl.BlockSpec(memory_space=pltpu.VMEM)
     far = pl.BlockSpec(memory_space=pl.ANY)
     return pl.pallas_call(
         functools.partial(block_body, planes),
         out_shape=pltpu.VMEM((tokens, width), bf16),
-        in_specs=[far] * 4 + [whole] * 3 + [far, whole, far, whole] + [far] * 3,
+        in_specs=[far] * 14,
         out_specs=whole,
         scratch_shapes=scratch,
         compiler_params=pltpu.CompilerParams(

time: 162 us -> 162 us (level)
  no operation moved by 1% of the time
where the time goes in v5:
time: 162 us; the launch traced here: 161 us
  Pallas kernels  160 us (99%)
    pallas_call x1, Pallas kernels, plane_layer(): pl.pallas_call(functools.partial(block_body, planes), out_shape=pltpu.VME...  160 us

profile of v5, /device:TPU:24, one launch (start us, length us, event | category | flops | bytes accessed | tf_op | source)
XLA Modules:
  0.0 161.4 jit_solution(16311556477227072487)
XLA Ops:
  0.0 160.4 %block.1 = bf16[1024,512]{1,0:T(8,128)(2,1)S(1)} custom-call(bf16[1024,256]{1,0:T(8,128)(2,1)} %q_in.1, bf16[1024,256]{1,0:T(8,128)(2,1)} %k_in.1, bf16[1024,512]{1,0:T(8,128)(2,1)} %v_in.1, bf16[1024,512]{1,0:T(8,128)(2,1)} %open_in.1, bf16[2,1024]{1,0:T(2,128)(2,1)} %input_far.1, bf16[2,1024]{1,0:T(2,128)(2,1)} %forget_far.1, f32[2,1024]{1,0:T(2,128)} %extra_far.1, ...), custom_call_target="tpu_custom_call" | custom-call | flops 22000001024 | bytes 10000000 | tf_op jit(solution)/shard_map/block/pallas_call | solution.py:1088
  160.4 1.0 copy.16

commit v6 on v5

--- a/solution.py
+++ b/solution.py
@@ -742,7 +742,7 @@
     z_forward(2, 2)
     z_down(1, 1)
 
-    short = 128
+    short = 256
 
     def norm_rows(owner, kinds):
         for kind in kinds:

time: 162 us -> 162 us (level)
  no operation moved by 1% of the time
where the time goes in v6:
time: 162 us; the launch traced here: 161 us
  Pallas kernels  160 us (99%)
    pallas_call x1, Pallas kernels, plane_layer(): pl.pallas_call(functools.partial(block_body, planes), out_shape=pltpu.VME...  160 us

profile of v6, /device:TPU:24, one launch (start us, length us, event | category | flops | bytes accessed | tf_op | source)
XLA Modules:
  0.0 161.4 jit_solution(5026627761913008439)
XLA Ops:
  0.0 160.4 %block.1 = bf16[1024,512]{1,0:T(8,128)(2,1)S(1)} custom-call(bf16[1024,256]{1,0:T(8,128)(2,1)} %q_in.1, bf16[1024,256]{1,0:T(8,128)(2,1)} %k_in.1, bf16[1024,512]{1,0:T(8,128)(2,1)} %v_in.1, bf16[1024,512]{1,0:T(8,128)(2,1)} %open_in.1, bf16[2,1024]{1,0:T(2,128)(2,1)} %input_far.1, bf16[2,1024]{1,0:T(2,128)(2,1)} %forget_far.1, f32[2,1024]{1,0:T(2,128)} %extra_far.1, ...), custom_call_target="tpu_custom_call" | custom-call | flops 22000001024 | bytes 10000000 | tf_op jit(solution)/shard_map/block/pallas_call | solution.py:1088
  160.4 1.0 copy.16
